TPU v7x, 128 devices: a whole 4x4x4 slice. The times are simulated.
128 devices in a mesh: sp: 32 (over z, y, core), tp: 4 (over x).
Axes of the slice: x: 4, y: 4, z: 4, core: 2. Of those that a mesh axis runs over, the one named last changes fastest.
Arguments:
- middle_stream: bfloat16 [6144, 2048], P('sp', 'tp'), may hold values from -6 to 6
- output_gradient: bfloat16 [6144, 2048], P('sp', 'tp'), may hold values from -6 to 6
- routes: int32 [6144, 2], P('sp'), may hold values from 0 to 31, all different within a row; in each aligned block of 192 rows (0 to 191, 192 to 383, ...) at most 18 rows name the same one
- chosen_expert_weight: float32 [6144, 2], P('sp'), may hold values from 0.2 to 1
- expert_gate_weight: bfloat16 [32, 2048, 3584], P('sp', None, 'tp'), may hold values from -0.125 to 0.125
- expert_up_weight: bfloat16 [32, 2048, 3584], P('sp', None, 'tp'), may hold values from -0.125 to 0.125
- expert_down_weight: bfloat16 [32, 3584, 2048], P('sp', 'tp'), may hold values from -0.09375 to 0.09375
- recurrent_output_weight: bfloat16 [2048, 1024], P(None, 'tp'), may hold values from -0.1875 to 0.1875
- recurrence_input: bfloat16 [6144, 1024], P('sp', 'tp'), may hold values from -8 to 8
- output_gate_logits: bfloat16 [6144, 1024], P('sp', 'tp'), may hold values from -6 to 6
- recurrence_gate_weight: bfloat16 [8, 128, 128], replicated, may hold values from -0.5 to 0.5
- input_gate_weight: bfloat16 [8, 128, 128], replicated, may hold values from -0.5 to 0.5
- channel_decay_param: float32 [1024], P('tp'), may hold values from 4 to 13
- extra_log_decay: float32 [6144, 1024], P('sp', 'tp'), may hold values from -0.7 to 0
Outputs:
- grad_gate: bfloat16 [32, 2048, 3584], P('sp', None, 'tp')
- grad_up: bfloat16 [32, 2048, 3584], P('sp', None, 'tp')
- grad_down: bfloat16 [32, 3584, 2048], P('sp', 'tp')
- grad_out_proj: float32 [2048, 1024], P('sp', 'tp')
- grad_input: float32 [6144, 1024], P('sp', 'tp')
- grad_gate_pre: float32 [6144, 1024], P('sp', 'tp')
Inputs may be any that keep to these rules, and one draw needn't show every extreme that they name: `routes`: in the rows of one index of sp no expert is named more than 18 times, a bound that some block reaches in some of them; the entries of a row differ.
All inputs are finite; a program needn't handle non-finite values.
Results may differ from a plain program's by a relative error of at most 0.017.
Values may be sent and summed in bfloat16 or wider, within the bound.
A program may use at most 128 MiB of HBM per device.

v0:
```python
import functools

import jax
import jax.numpy as jnp
from jax import lax
from jax.experimental import pallas as pl
from jax.experimental.pallas import tpu as pltpu
from jax.sharding import PartitionSpec as P

BF16 = jnp.bfloat16
F32 = jnp.float32
MESH = pl.DeviceIdType.MESH
LANE = 128
MAIN = 16


def mm(a, b, ca=1, cb=0):
    return lax.dot_general(a, b, (((ca,), (cb,)), ((), ())), preferred_element_type=F32)


def iota(shape, dim):
    return lax.broadcasted_iota(jnp.int32, shape, dim).astype(F32)


def copy_to(src, dst, send_sem, recv_sem, sp, tp):
    return pltpu.make_async_remote_copy(
        src_ref=src,
        dst_ref=dst,
        send_sem=send_sem,
        recv_sem=recv_sem,
        device_id=(sp, tp),
        device_id_type=MESH,
    )


def greet(targets):
    barrier = pltpu.get_barrier_semaphore()
    for sp, tp in targets:
        pl.semaphore_signal(barrier, inc=1, device_id=(sp, tp), device_id_type=MESH)


def met(count):
    pl.semaphore_wait(pltpu.get_barrier_semaphore(), count)


def shifted(value, by, fill, row):
    rows = value.shape[0]
    if by > 0:
        return jnp.where(row >= by, pltpu.roll(value, by, 0), fill)
    return jnp.where(row < rows + by, pltpu.roll(value, rows + by, 0), fill)


def scan_rows(gain, value, sign):
    rows = value.shape[0]
    row = lax.broadcasted_iota(jnp.int32, value.shape, 0)
    step = 1
    while step < rows:
        value = value + gain * shifted(value, sign * step, 0.0, row)
        gain = gain * shifted(gain, sign * step, 1.0, row)
        step *= 2
    return gain, value


def log1p_of(z):
    series = z * (1.0 - z * (0.5 - z * (1.0 / 3.0 - z * (0.25 - z * (0.2 - z / 6.0)))))
    return jnp.where(z < 0.03, series, jnp.log(1.0 + z))


def one_less_exp(y):
    part = 1.0 + y / 7.0
    for k in (6.0, 5.0, 4.0, 3.0, 2.0):
        part = 1.0 + (y / k) * part
    return jnp.where(y > -0.5, -y * part, 1.0 - jnp.exp(y))


def gelu_both(x):
    c = 0.7978845608028654
    t = jnp.tanh(c * (x + 0.044715 * x * x * x))
    value = 0.5 * x * (1.0 + t)
    slope = 0.5 * (1.0 + t) + 0.5 * x * (1.0 - t * t) * c * (1.0 + 3.0 * 0.044715 * x * x)
    return value, slope


def dispatch_kernel(
    n_sp,
    x_ref,
    g_ref,
    rt_ref,
    wt_ref,
    u_ref,
    ogl_ref,
    wr_ref,
    wi_ref,
    cdp_ref,
    eld_ref,
    rows_ref,
    cot_ref,
    rec_ref,
    lru_ref,
    gain_ref,
    send,
    recv,
    ext,
    stat,
    stats,
    d_send,
    d_recv,
    own_sem,
    r_send,
    l_send,
    y_send,
    fl_recv,
    fr_recv,
    ff_recv,
    s_send,
    s_recv,
):
    me, tp = lax.axis_index("sp"), lax.axis_index("tp")
    right, left, far = (lax.rem(tp + k, 4) for k in (1, 3, 2))
    tokens, feat = x_ref.shape
    extra = 2
    groups = 8
    per = n_sp // groups
    greet([(lax.rem(me + d, n_sp), tp) for d in range(1, n_sp)] + [(me, right), (me, left)])

    r0 = rt_ref[0:1, :].astype(F32)
    r1 = rt_ref[1:2, :].astype(F32)
    w0 = wt_ref[0:1, :]
    w1 = wt_ref[1:2, :]
    expert = iota((n_sp, tokens), 0)
    h0 = expert == r0
    h1 = expert == r1
    held = (h0 | h1).astype(F32).astype(BF16)
    before = (iota((tokens, tokens), 0) < iota((tokens, tokens), 1)).astype(F32).astype(BF16)
    rank = mm(held, before)
    k0 = jnp.sum(jnp.where(h0, rank, 0.0), axis=0, keepdims=True)
    k1 = jnp.sum(jnp.where(h1, rank, 0.0), axis=0, keepdims=True)
    m0 = jnp.where(k0 < MAIN, r0 * MAIN + k0, -1.0)
    m1 = jnp.where(k1 < MAIN, r1 * MAIN + k1, -1.0)
    e0 = jnp.where(k0 < MAIN, -1.0, r0 * extra + k0 - MAIN)
    e1 = jnp.where(k1 < MAIN, -1.0, r1 * extra + k1 - MAIN)
    x = x_ref[...]
    g = g_ref[...]
    block = 128
    for at in range(0, n_sp * MAIN, block):
        slot = iota((block, tokens), 0) + float(at)
        p0 = slot == m0
        p1 = slot == m1
        pick = (p0 | p1).astype(F32).astype(BF16)
        weight = jnp.sum(jnp.where(p0, w0, 0.0) + jnp.where(p1, w1, 0.0), axis=1, keepdims=True)
        send[at : at + block, 0:feat] = mm(pick, x).astype(BF16)
        send[at : at + block, feat : 2 * feat] = (mm(pick, g) * weight).astype(BF16)
    slot = iota((n_sp * extra, tokens), 0)
    p0 = slot == e0
    p1 = slot == e1
    pick = (p0 | p1).astype(F32).astype(BF16)
    weight = jnp.sum(jnp.where(p0, w0, 0.0) + jnp.where(p1, w1, 0.0), axis=1, keepdims=True)
    ex = mm(pick, x)
    eg = mm(pick, g) * weight
    cuts = feat // LANE
    for b in range(cuts):
        ext[pl.ds(b, n_sp * extra, stride=2 * cuts), :] = ex[:, b * LANE : (b + 1) * LANE]
        ext[pl.ds(cuts + b, n_sp * extra, stride=2 * cuts), :] = eg[:, b * LANE : (b + 1) * LANE]
    send[:, 2 * feat : 2 * feat + LANE] = ext[...].astype(BF16)

    met(n_sp + 1)

    def dispatch(peer, sem):
        return copy_to(
            send.at[pl.ds(pl.multiple_of(peer * MAIN, MAIN), MAIN)],
            recv.at[tp, pl.ds(pl.multiple_of(me * MAIN, MAIN), MAIN)],
            d_send.at[sem],
            d_recv.at[me],
            peer,
            tp,
        )

    def arrival(source):
        return copy_to(
            send.at[pl.ds(0, MAIN)],
            recv.at[tp, pl.ds(pl.multiple_of(source * MAIN, MAIN), MAIN)],
            d_send.at[0],
            d_recv.at[source],
            source,
            tp,
        )

    own = pltpu.make_async_copy(
        send.at[pl.ds(pl.multiple_of(me * MAIN, MAIN), MAIN)],
        recv.at[tp, pl.ds(pl.multiple_of(me * MAIN, MAIN), MAIN)],
        own_sem,
    )
    own.start()
    sends = [dispatch(lax.rem(me + n_sp - d, n_sp), d) for d in range(1, n_sp)]
    for s in sends:
        s.start()

    u = u_ref[...]
    uf = u.astype(F32)
    blocks = u.shape[1] // LANE
    pre_r = []
    pre_i = []
    for b in range(blocks):
        ub = u[:, b * LANE : (b + 1) * LANE]
        pre_r.append(mm(ub, wr_ref[tp * blocks + b]))
        pre_i.append(mm(ub, wi_ref[tp * blocks + b]))
    forget = jax.nn.sigmoid(jnp.concatenate(pre_r, axis=1))
    admit = jax.nn.sigmoid(jnp.concatenate(pre_i, axis=1))
    p = cdp_ref[...]
    base = jnp.maximum(-p, 0.0) + log1p_of(jnp.exp(-jnp.abs(p)))
    log_decay = -8.0 * forget * base + eld_ref[...]
    decay = jnp.exp(log_decay)
    scale = jnp.sqrt(one_less_exp(2.0 * log_decay))
    gain, local = scan_rows(decay, uf * admit * scale, 1)
    stat[0, 0:1, :] = gain[tokens - 1 : tokens, :]
    stat[0, 1:2, :] = local[tokens - 1 : tokens, :]
    stats[me, 0:1, :] = gain[tokens - 1 : tokens, :]
    stats[me, 1:2, :] = local[tokens - 1 : tokens, :]
    told = [
        copy_to(
            stat.at[0], stats.at[me], s_send.at[d], s_recv.at[me], lax.rem(me + n_sp - d, n_sp), tp
        )
        for d in range(1, n_sp)
    ]
    for s in told:
        s.start()

    size = per * MAIN
    g0 = me // per

    def span(i):
        start = lax.rem(g0 + i, groups) * size
        return pl.ds(pl.multiple_of(start, size), size)

    def pass_on(quarter, i, send_sem, recv_sem, to):
        return copy_to(
            recv.at[quarter, span(i)], recv.at[quarter, span(i)], send_sem, recv_sem, me, to
        )

    started = []

    def relay(i):
        if i % 2 == 0:
            pass_on(left, i, l_send.at[i], fl_recv.at[i], right).wait_recv()
            c = pass_on(left, i, y_send.at[i], ff_recv.at[i], right)
        else:
            pass_on(right, i, r_send.at[i], fr_recv.at[i], left).wait_recv()
            c = pass_on(right, i, y_send.at[i], ff_recv.at[i], left)
        c.start()
        started.append(c)

    for i in range(groups):
        if i == 0:
            own.wait()
        for k in range(per):
            source = lax.rem(g0 + i, groups) * per + k
            if i == 0:

                @pl.when(source != me)
                def _():
                    arrival(source).wait_recv()
            else:
                arrival(source).wait_recv()
        for c in (
            pass_on(tp, i, r_send.at[i], fl_recv.at[i], right),
            pass_on(tp, i, l_send.at[i], fr_recv.at[i], left),
        ):
            c.start()
            started.append(c)
        if i > 0:
            relay(i - 1)

    for d in range(1, n_sp):
        source = lax.rem(me + d, n_sp)
        copy_to(stat.at[0], stats.at[source], s_send.at[0], s_recv.at[source], source, tp).wait_recv()
    carry = jnp.zeros((1, u.shape[1]), F32)
    for s in range(n_sp):
        carry = jnp.where(s < me, stats[s, 0:1, :] * carry + stats[s, 1:2, :], carry)
    gain_ref[...] = stats[...]
    states = local + gain * carry
    row = lax.broadcasted_iota(jnp.int32, states.shape, 0)
    prev = jnp.where(row == 0, carry, pltpu.roll(states, 1, 0))
    gelu, slope = gelu_both(ogl_ref[...].astype(F32))
    lru_ref[...] = (states * gelu).astype(BF16)
    rec_ref[0] = decay
    rec_ref[1] = gelu
    rec_ref[2] = states * slope
    rec_ref[3] = admit * scale
    rec_ref[4] = (
        (prev * decay - uf * admit * decay * decay / scale) * (-8.0 * base) * forget * (1.0 - forget)
    )
    rec_ref[5] = uf * scale * admit * (1.0 - admit)

    relay(groups - 1)
    for i in range(groups):
        if i % 2 == 1:
            pass_on(left, i, l_send.at[i], fl_recv.at[i], right).wait_recv()
        else:
            pass_on(right, i, r_send.at[i], fr_recv.at[i], left).wait_recv()
    for i in range(groups):
        pass_on(far, i, y_send.at[i], ff_recv.at[i], right).wait_recv()

    for q in range(4):
        rows_ref[0 : n_sp * MAIN, q * feat : (q + 1) * feat] = recv[q, :, 0:feat]
        cot_ref[0 : n_sp * MAIN, q * feat : (q + 1) * feat] = recv[q, :, feat : 2 * feat]
        ext[...] = recv[q, :, 2 * feat : 2 * feat + LANE].astype(F32)
        for b in range(cuts):
            at = q * feat + b * LANE
            rows_ref[n_sp * MAIN :, at : at + LANE] = ext[
                pl.ds(b, n_sp * extra, stride=2 * cuts), :
            ].astype(BF16)
            cot_ref[n_sp * MAIN :, at : at + LANE] = ext[
                pl.ds(cuts + b, n_sp * extra, stride=2 * cuts), :
            ].astype(BF16)

    for c in sends + told + started:
        c.wait_send()


def dispatch(n_sp, x, g, rt, wt, u, ogl, wr, wi, cdp, eld):
    tokens, feat = x.shape
    chans = u.shape[1]
    slots = n_sp * (MAIN + 2)
    width = 2 * feat + LANE
    vmem = pl.BlockSpec(memory_space=pltpu.VMEM)
    dma = pltpu.SemaphoreType.DMA
    return pl.pallas_call(
        functools.partial(dispatch_kernel, n_sp),
        out_shape=(
            jax.ShapeDtypeStruct((slots, 4 * feat), BF16),
            jax.ShapeDtypeStruct((slots, 4 * feat), BF16),
            jax.ShapeDtypeStruct((6, tokens, chans), F32),
            jax.ShapeDtypeStruct((tokens, chans), BF16),
            jax.ShapeDtypeStruct((n_sp, 2, chans), F32),
        ),
        in_specs=[vmem] * 10,
        out_specs=(vmem,) * 5,
        scratch_shapes=[
            pltpu.VMEM((n_sp * MAIN, width), BF16),
            pltpu.VMEM((4, n_sp * MAIN, width), BF16),
            pltpu.VMEM((n_sp * MAIN, LANE), F32),
            pltpu.VMEM((1, 2, chans), F32),
            pltpu.VMEM((n_sp, 2, chans), F32),
            dma((n_sp,)),
            dma((n_sp,)),
            dma,
            dma((8,)),
            dma((8,)),
            dma((8,)),
            dma((8,)),
            dma((8,)),
            dma((8,)),
            dma((n_sp,)),
            dma((n_sp,)),
        ],
        compiler_params=pltpu.CompilerParams(
            collective_id=0, has_side_effects=True, vmem_limit_bytes=60 * 1024 * 1024
        ),
        name="dispatch",
    )(x, g, rt, wt, u, ogl, wr, wi, cdp, eld)


def tail_kernel(
    n_sp,
    sg_ref,
    og_ref,
    routes_ref,
    wout_ref,
    wr_ref,
    wi_ref,
    rec_ref,
    lru_ref,
    gain_ref,
    gop_ref,
    gin_ref,
    ggp_ref,
    rext,
    arr,
    arrx,
    full,
    prod,
    pair,
    summed,
    owned,
    term,
    terms,
    m_send,
    m_recv,
    x_send,
    x_recv,
    own_sems,
    a_send,
    fl_recv,
    fr_recv,
    ff_recv,
    p_sems,
    o_send,
    o_recv,
    t_send,
    t_recv,
):
    me, tp = lax.axis_index("sp"), lax.axis_index("tp")
    right, left, far = (lax.rem(tp + k, 4) for k in (1, 3, 2))
    core = lax.rem(me, 2)
    chip = me // 2
    partner = me + 1 - 2 * core
    chips = n_sp // 2
    tokens, feat = og_ref.shape
    extra = 2
    cuts = feat // LANE
    xrows = extra * cuts
    greet([(lax.rem(me + d, n_sp), tp) for d in range(1, n_sp)] + [(me, right), (me, left)])

    main = n_sp * MAIN
    sx = sg_ref[main:, :].astype(F32)
    for b in range(cuts):
        rext[pl.ds(b, n_sp * extra, stride=cuts), :] = sx[:, b * LANE : (b + 1) * LANE]
    r0 = routes_ref[:, 0:1].astype(F32)
    r1 = routes_ref[:, 1:2].astype(F32)
    expert = iota((tokens, n_sp), 1)
    h0 = expert == r0
    h1 = expert == r1
    held = (h0 | h1).astype(F32).astype(BF16)
    before = (iota((tokens, tokens), 1) < iota((tokens, tokens), 0)).astype(F32).astype(BF16)
    rank = mm(before, held)
    k0 = jnp.sum(jnp.where(h0, rank, 0.0), axis=1, keepdims=True)
    k1 = jnp.sum(jnp.where(h1, rank, 0.0), axis=1, keepdims=True)
    m0 = jnp.where(k0 < MAIN, r0 * MAIN + k0, -1.0)
    m1 = jnp.where(k1 < MAIN, r1 * MAIN + k1, -1.0)
    e0 = jnp.where(k0 < MAIN, -1.0, r0 * extra + k0 - MAIN)
    e1 = jnp.where(k1 < MAIN, -1.0, r1 * extra + k1 - MAIN)
    slot = iota((tokens, main), 1)
    pick = ((slot == m0) | (slot == m1)).astype(F32).astype(BF16)
    slot = iota((tokens, n_sp * extra), 1)
    pickx = ((slot == e0) | (slot == e1)).astype(F32).astype(BF16)

    met(n_sp + 1)

    def rows_of(index, size):
        return pl.ds(pl.multiple_of(index * size, size), size)

    own = [
        pltpu.make_async_copy(
            sg_ref.at[rows_of(me, MAIN)], arr.at[rows_of(me, MAIN)], own_sems.at[0]
        ),
        pltpu.make_async_copy(
            rext.at[rows_of(me, xrows)], arrx.at[rows_of(me, xrows)], own_sems.at[1]
        ),
    ]
    sends = []
    for d in range(1, n_sp):
        peer = lax.rem(me + d, n_sp)
        sends.append(
            copy_to(
                sg_ref.at[rows_of(peer, MAIN)],
                arr.at[rows_of(me, MAIN)],
                m_send.at[d],
                m_recv.at[me],
                peer,
                tp,
            )
        )
        sends.append(
            copy_to(
                rext.at[rows_of(peer, xrows)],
                arrx.at[rows_of(me, xrows)],
                x_send.at[d],
                x_recv.at[me],
                peer,
                tp,
            )
        )
    for c in own + sends:
        c.start()
    for c in own:
        c.wait()
    for d in range(1, n_sp):
        source = lax.rem(me + n_sp - d, n_sp)
        copy_to(
            sg_ref.at[rows_of(source, MAIN)],
            arr.at[rows_of(source, MAIN)],
            m_send.at[d],
            m_recv.at[source],
            source,
            tp,
        ).wait_recv()
        copy_to(
            rext.at[rows_of(source, xrows)],
            arrx.at[rows_of(source, xrows)],
            x_send.at[d],
            x_recv.at[source],
            source,
            tp,
        ).wait_recv()
    back = mm(pick, arr[...])
    backx = jnp.concatenate(
        [mm(pickx, arrx[pl.ds(b, n_sp * extra, stride=cuts), :].astype(BF16)) for b in range(cuts)],
        axis=1,
    )
    full[tp] = (og_ref[...].astype(F32) + (back + backx)).astype(BF16)

    half = tokens // 2

    def piece(quarter, h, send_sem, recv_sem, to):
        ref = full.at[quarter, pl.ds(h * half, half)]
        return copy_to(ref, ref, send_sem, recv_sem, me, to)

    for h in (0, 1):
        sends.append(piece(tp, h, a_send.at[h], fl_recv.at[h], right))
        sends.append(piece(tp, 1 - h, a_send.at[3 - h], fr_recv.at[1 - h], left))
        sends[-2].start()
        sends[-1].start()

    lru = lru_ref[...]

    def use(quarter):
        part = full[quarter]
        wide = mm(part, lru, 0, 0).astype(BF16)
        prod[pl.ds(quarter * (chips // 4), chips // 4)] = wide.reshape(
            chips // 4, 2, wide.shape[0] // (chips // 2), wide.shape[1]
        )
        return mm(part, wout_ref[pl.ds(pl.multiple_of(quarter * feat, feat), feat), :])

    mixer = use(tp)
    piece(left, 0, a_send.at[0], fl_recv.at[0], right).wait_recv()
    sends.append(piece(left, 0, a_send.at[4], ff_recv.at[0], right))
    sends[-1].start()
    piece(right, 1, a_send.at[0], fr_recv.at[1], left).wait_recv()
    sends.append(piece(right, 1, a_send.at[5], ff_recv.at[1], left))
    sends[-1].start()
    piece(left, 1, a_send.at[0], fl_recv.at[1], right).wait_recv()
    mixer = mixer + use(left)
    piece(right, 0, a_send.at[0], fr_recv.at[0], left).wait_recv()
    mixer = mixer + use(right)
    piece(far, 0, a_send.at[0], ff_recv.at[0], right).wait_recv()
    piece(far, 1, a_send.at[0], ff_recv.at[1], left).wait_recv()
    mixer = mixer + use(far)

    trade = copy_to(prod.at[:, 1 - core], pair, p_sems.at[0], p_sems.at[1], partner, tp)
    trade.start()

    decay = rec_ref[0]
    row = lax.broadcasted_iota(jnp.int32, decay.shape, 0)
    ggp_ref[...] = mixer * rec_ref[2]
    gain, tail = scan_rows(shifted(decay, -1, 1.0, row), mixer * rec_ref[1], -1)
    last = decay[0:1, :] * tail[0:1, :]
    term[0] = last
    terms[me] = last
    for d in range(1, n_sp):
        sends.append(
            copy_to(
                term.at[0], terms.at[me], t_send.at[d], t_recv.at[me], lax.rem(me + d, n_sp), tp
            )
        )
        sends[-1].start()

    trade.wait()
    summed[...] = (prod[:, core].astype(F32) + pair[...].astype(F32)).astype(BF16)
    for d in range(1, chips):
        to = lax.rem(chip + d, chips)
        sends.append(
            copy_to(
                summed.at[to], owned.at[chip], o_send.at[d], o_recv.at[chip], to * 2 + core, tp
            )
        )
        sends[-1].start()
    owned[chip] = summed[chip]

    for d in range(1, n_sp):
        source = lax.rem(me + n_sp - d, n_sp)
        copy_to(term.at[0], terms.at[source], t_send.at[d], t_recv.at[source], source, tp).wait_recv()
    later = jnp.zeros_like(last)
    for s in range(n_sp - 1, -1, -1):
        later = jnp.where(s > me, gain_ref[s, 0:1, :] * later + terms[s], later)
    grad = tail + gain * later
    d_recall = (grad * rec_ref[4]).astype(BF16)
    d_admit = (grad * rec_ref[5]).astype(BF16)
    direct = grad * rec_ref[3]
    blocks = direct.shape[1] // LANE
    for b in range(blocks):
        cols = slice(b * LANE, (b + 1) * LANE)
        gin_ref[:, cols] = (
            direct[:, cols]
            + mm(d_recall[:, cols], wr_ref[tp * blocks + b], 1, 1)
            + mm(d_admit[:, cols], wi_ref[tp * blocks + b], 1, 1)
        )

    for d in range(1, chips):
        source = lax.rem(chip + chips - d, chips)
        copy_to(
            summed.at[source],
            owned.at[source],
            o_send.at[d],
            o_recv.at[source],
            source * 2 + core,
            tp,
        ).wait_recv()
    total = owned[0].astype(F32)
    for j in range(1, chips):
        total = total + owned[j].astype(F32)
    gop_ref[...] = total
    for c in sends:
        c.wait_send()


def tail(n_sp, sg, og, routes, wout, wr, wi, rec, lru, gains):
    tokens, feat = og.shape
    chans = lru.shape[1]
    chips = n_sp // 2
    share = wout.shape[0] // n_sp
    vmem = pl.BlockSpec(memory_space=pltpu.VMEM)
    dma = pltpu.SemaphoreType.DMA
    xrows = 2 * feat // LANE
    return pl.pallas_call(
        functools.partial(tail_kernel, n_sp),
        out_shape=(
            jax.ShapeDtypeStruct((share, chans), F32),
            jax.ShapeDtypeStruct((tokens, chans), F32),
            jax.ShapeDtypeStruct((tokens, chans), F32),
        ),
        in_specs=[vmem] * 9,
        out_specs=(vmem,) * 3,
        scratch_shapes=[
            pltpu.VMEM((n_sp * xrows, LANE), F32),
            pltpu.VMEM((n_sp * MAIN, feat), BF16),
            pltpu.VMEM((n_sp * xrows, LANE), F32),
            pltpu.VMEM((4, tokens, feat), BF16),
            pltpu.VMEM((chips, 2, share, chans), BF16),
            pltpu.VMEM((chips, share, chans), BF16),
            pltpu.VMEM((chips, share, chans), BF16),
            pltpu.VMEM((chips, share, chans), BF16),
            pltpu.VMEM((1, 1, chans), F32),
            pltpu.VMEM((n_sp, 1, chans), F32),
            dma((n_sp,)),
            dma((n_sp,)),
            dma((n_sp,)),
            dma((n_sp,)),
            dma((2,)),
            dma((6,)),
            dma((2,)),
            dma((2,)),
            dma((2,)),
            dma((2,)),
            dma((chips,)),
            dma((chips,)),
            dma((n_sp,)),
            dma((n_sp,)),
        ],
        compiler_params=pltpu.CompilerParams(
            collective_id=1, has_side_effects=True, vmem_limit_bytes=40 * 1024 * 1024
        ),
        name="tail",
    )(sg, og, routes, wout, wr, wi, rec, lru, gains)


def summed_over_tp(parts):
    fwd = [(k, (k + 1) % 4) for k in range(4)]
    bwd = [(k, (k + 3) % 4) for k in range(4)]
    here, right, far, left = parts
    half = here.shape[0] // 2
    far_a = lax.ppermute(far[:half], "tp", fwd)
    far_b = lax.ppermute(far[half:], "tp", bwd)
    right_b = lax.ppermute(right[half:], "tp", fwd)
    left_a = lax.ppermute(left[:half], "tp", bwd)
    right_a = lax.ppermute((right[:half].astype(F32) + far_a.astype(F32)).astype(BF16), "tp", fwd)
    left_b = lax.ppermute((left[half:].astype(F32) + far_b.astype(F32)).astype(BF16), "tp", bwd)
    top = here[:half].astype(F32) + (right_a.astype(F32) + left_a.astype(F32))
    low = here[half:].astype(F32) + (right_b.astype(F32) + left_b.astype(F32))
    return jnp.concatenate([top, low], axis=0).astype(BF16)


def per_device(
    n_sp,
    middle_stream,
    output_gradient,
    routes,
    chosen_expert_weight,
    expert_gate_weight,
    expert_up_weight,
    expert_down_weight,
    recurrent_output_weight,
    recurrence_input,
    output_gate_logits,
    recurrence_gate_weight,
    input_gate_weight,
    channel_decay_param,
    extra_log_decay,
):
    feat = middle_stream.shape[1]
    inputs, cotangent, rec, lru, gains = dispatch(
        n_sp,
        middle_stream,
        output_gradient,
        routes.T,
        chosen_expert_weight.T,
        recurrence_input,
        output_gate_logits,
        recurrence_gate_weight,
        input_gate_weight,
        channel_decay_param[None],
        extra_log_decay,
    )
    gate_weight, up_weight, down_weight = (
        expert_gate_weight[0],
        expert_up_weight[0],
        expert_down_weight[0],
    )
    gate_act = mm(inputs, gate_weight)
    up_act = mm(inputs, up_weight)
    sigmoid_gate = jax.nn.sigmoid(gate_act)
    silu_act = gate_act * sigmoid_gate
    hidden = (silu_act * up_act).astype(BF16)
    d_hidden = mm(cotangent, down_weight, 1, 1)
    d_gate = (d_hidden * up_act * sigmoid_gate * (1.0 + gate_act * (1.0 - sigmoid_gate))).astype(
        BF16
    )
    d_up = (d_hidden * silu_act).astype(BF16)
    partial = (mm(d_gate, gate_weight, 1, 1) + mm(d_up, up_weight, 1, 1)).astype(BF16)
    tp = lax.axis_index("tp")
    parts = [
        lax.dynamic_slice_in_dim(partial, lax.rem(tp + k, 4) * feat, feat, 1) for k in range(4)
    ]
    slot_grad = summed_over_tp(parts)
    grad_down = mm(hidden, cotangent, 0, 0).astype(BF16)
    grad_gate = mm(inputs, d_gate, 0, 0).astype(BF16)
    grad_up = mm(inputs, d_up, 0, 0).astype(BF16)
    grad_out_proj, grad_input, grad_gate_pre = tail(
        n_sp,
        slot_grad,
        output_gradient,
        routes,
        recurrent_output_weight,
        recurrence_gate_weight,
        input_gate_weight,
        rec,
        lru,
        gains,
    )
    return (
        grad_gate[None],
        grad_up[None],
        grad_down[None],
        grad_out_proj,
        grad_input,
        grad_gate_pre,
    )


def solution(mesh):
    placed = (
        P("sp", "tp"),
        P("sp", "tp"),
        P("sp", None),
        P("sp", None),
        P("sp", None, "tp"),
        P("sp", None, "tp"),
        P("sp", "tp", None),
        P(None, "tp"),
        P("sp", "tp"),
        P("sp", "tp"),
        P(),
        P(),
        P("tp"),
        P("sp", "tp"),
    )
    return jax.shard_map(
        functools.partial(per_device, mesh.shape["sp"]),
        mesh=mesh,
        in_specs=placed,
        out_specs=(
            P("sp", None, "tp"),
            P("sp", None, "tp"),
            P("sp", "tp", None),
            P("sp", "tp"),
            P("sp", "tp"),
            P("sp", "tp"),
        ),
        check_vma=False,
    )
```

profile of v0, /device:TPU:27, one launch (start us, length us, event | category | flops | bytes accessed | tf_op | source)
XLA Modules:
  0.0 161.9 jit_solution(3274579803104572194)
XLA Ops:
  0.7 66.1 %dispatch.1 = (bf16[576,2048]{1,0:T(8,128)(2,1)}, bf16[576,2048]{1,0:T(8,128)(2,1)}, f32[6,192,256]{2,1,0:T(8,128)}, bf16[192,256]{1,0:T(8,128)(2,1)}, f32[32,2,256]{2,1,0:T(2,128)}) custom-call(bf16[192,512]{1,0:T(8,128)(2,1)} %x_ref.1, bf16[192,512]{1,0:T(8,128)(2,1)} %og_ref.1, s32[2,192]{1,0:T(2,128)} %bitcast.36, f32[2,192]{1,0:T(2,128)} %bitcast.37, ...), custom_call_target="tpu_custom_call" | custom-call | tf_op jit(solution)/shard_map/dispatch/pallas_call | solution.py:327
  66.8 0.0 copy-start.10
  66.8 5.5 %fusion.2 = f32[576,896]{1,0:T(8,128)S(1)} fusion(bf16[576,2048]{1,0:T(8,128)(2,1)} %get-tuple-element.14, bf16[1,2048,896]{2,1,0:T(8,128)(2,1)} %param.18), kind=kOutput, calls=%fused_computation.3 | convolution fusion | flops 2113929216 | bytes 8093696 | tf_op jit(solution)/shard_map/dot_general | solution.py:18
  72.3 0.0 copy-start.17
  72.3 0.0 copy-start.8
  72.3 2.6 %fusion.6 = f32[576,896]{1,0:T(8,128)S(1)} fusion(bf16[576,2048]{1,0:T(8,128)(2,1)S(1)} %copy-done.11, bf16[1,2048,896]{2,1,0:T(8,128)(2,1)S(1)} %copy-done.10), kind=kOutput, calls=%fused_computation.7 | convolution fusion | flops 2113929216 | bytes 8093696 | tf_op jit(solution)/shard_map/dot_general | solution.py:18
  75.0 0.1 copy-done.8
  75.1 0.7 copy-done.13
  75.8 3.2 %multiply_convert_fusion.1 = (bf16[576,896]{1,0:T(8,128)(2,1)S(1)}, bf16[576,896]{1,0:T(8,128)(2,1)S(1)}) fusion(f32[576,896]{1,0:T(8,128)S(1)} %fusion.2, f32[576,896]{1,0:T(8,128)S(1)} %fusion.6, bf16[576,2048]{1,0:T(8,128)(2,1)S(1)} %copy-done.13, bf16[1,896,2048]{2,1,0:T(8,128)(2,1)S(1)} %copy-done.8), kind=kOutput, calls=%fused_computation.15 | convolution fusion | flops 2120638464 | bytes 12222464 | tf_op jit(solution)/shard_map/dot_general | solution.py:18
  79.1 0.9 copy-done.15
  80.0 4.3 %fusion = f32[576,2048]{1,0:T(8,128)} fusion(bf16[576,896]{1,0:T(8,128)(2,1)S(1)} %get-tuple-element.23, bf16[1,2048,896]{2,1,0:T(8,128)(2,1)S(1)} %copy-done.9), kind=kOutput, calls=%fused_computation.1 | convolution fusion | flops 2113929216 | bytes 9420800 | tf_op jit(solution)/shard_map/dot_general | solution.py:18
  84.3 5.8 %add_convert_fusion = bf16[576,2048]{1,0:T(8,128)(2,1)S(1)} fusion(f32[576,2048]{1,0:T(8,128)} %fusion, bf16[576,896]{1,0:T(8,128)(2,1)S(1)} %get-tuple-element.22, bf16[1,2048,896]{2,1,0:T(8,128)(2,1)} %param.19), kind=kOutput, calls=%fused_computation | convolution fusion | flops 2116288512 | bytes 11780096 | tf_op jit(solution)/shard_map/dot_general | solution.py:18
  90.2 1.0 constant_dynamic-slice_fusion
  91.2 1.5 collective-permute-start.2
  92.6 2.2 %collective-permute-start.4 = (bf16[288,512]{1,0:T(8,128)(2,1)}, bf16[288,512]{1,0:T(8,128)(2,1)}, u32[]{:S(2)}, u32[]{:S(2)}) collective-permute-start(bf16[288,512]{1,0:T(8,128)(2,1)} %get-tuple-element.28), channel_id=1, source_target_pairs={{0,3},{1,0},{2,1},{3,2},{4,7},{5,4},{6,5},{7,6},{8,11},{9,8},{10,9... | collective-permute-start | bytes 884744 | tf_op jit(solution)/shard_map/ppermute | solution.py:662
  94.8 4.7 %convert_bitcast_fusion = bf16[1,896,2048]{2,1,0:T(8,128)(2,1)} fusion(bf16[576,2048]{1,0:T(8,128)(2,1)S(1)} %copy-done.14, f32[576,896]{1,0:T(8,128)S(1)} %copy-done.20, f32[576,896]{1,0:T(8,128)S(1)} %copy-done.18), kind=kOutput, calls=%fused_computation.11 | convolution fusion | flops 2118860800 | bytes 10158080 | tf_op jit(solution)/shard_map/dot_general | solution.py:18
  99.5 0.1 copy.20.routes_ref
  99.6 0.1 add_convert_fusion.4
  99.7 0.1 collective-permute-start.1
  99.8 7.3 %convert_bitcast_fusion.1 = bf16[1,2048,896]{2,1,0:T(8,128)(2,1)} fusion(bf16[576,2048]{1,0:T(8,128)(2,1)} %get-tuple-element.14, bf16[576,896]{1,0:T(8,128)(2,1)} %copy-done.21), kind=kOutput, calls=%fused_computation.12 | convolution fusion | flops 2115764224 | bytes 7061504 | tf_op jit(solution)/shard_map/dot_general | solution.py:18
  107.1 3.0 %collective-permute-done.1 = bf16[288,512]{1,0:T(8,128)(2,1)S(1)} collective-permute-done((bf16[288,512]{1,0:T(8,128)(2,1)S(1)}, bf16[288,512]{1,0:T(8,128)(2,1)S(1)}, u32[]{:S(2)}, u32[]{:S(2)}) %collective-permute-start.1) | collective-permute-done | bytes 294944 | tf_op jit(solution)/shard_map/ppermute | solution.py:665
  110.1 1.3 add_convert_fusion.3
  111.4 3.2 %collective-permute-start.5 = (bf16[288,512]{1,0:T(8,128)(2,1)S(1)}, bf16[288,512]{1,0:T(8,128)(2,1)S(1)}, u32[]{:S(2)}, u32[]{:S(2)}) collective-permute-start(bf16[288,512]{1,0:T(8,128)(2,1)S(1)} %get-tuple-element.25), channel_id=1, source_target_pairs={{0,3},{1,0},{2,1},{3,2},{4,7},{5,4},{6,5},{7,6},{8,11},{9,8},{10,9... | collective-permute-start | bytes 884744 | tf_op jit(solution)/shard_map/ppermute | solution.py:666
  114.6 0.0 copy-start.4
  114.6 4.8 %convert_bitcast_fusion.2 = bf16[1,2048,896]{2,1,0:T(8,128)(2,1)} fusion(bf16[576,2048]{1,0:T(8,128)(2,1)S(1)} %copy-done.12, bf16[576,896]{1,0:T(8,128)(2,1)S(1)} %copy-done.16), kind=kOutput, calls=%fused_computation.13 | convolution fusion | flops 2115764224 | bytes 7061504 | tf_op jit(solution)/shard_map/dot_general | solution.py:18
  119.5 0.1 add_convert_fusion.1
  119.7 1.0 copy-done
  120.7 0.3 copy-done.1
  121.1 38.8 %tail.1 = (f32[64,256]{1,0:T(8,128)S(1)}, f32[192,256]{1,0:T(8,128)S(1)}, f32[192,256]{1,0:T(8,128)S(1)}) custom-call(bf16[576,512]{1,0:T(8,128)(2,1)S(1)} %pad_maximum_fusion.sg_ref, bf16[192,512]{1,0:T(8,128)(2,1)S(1)} %copy-done.4, s32[192,2]{1,0:T(8,128)S(1)} %copy.20.routes_ref, bf16[2048,256]{1,0:T(8,128)(2,1)S(1)} %copy-done.1, ...), custom_call_target="tpu_custom_call" | custom-call | tf_op jit(solution)/shard_map/tail/pallas_call | solution.py:614
  159.9 0.6 copy.24
  160.5 0.7 copy.25
  161.2 0.7 copy.26
  (43 shorter events, 0.1 us)
Async XLA Ops:
  66.8 5.5 %copy-start.10 = (bf16[1,2048,896]{2,1,0:T(8,128)(2,1)S(1)}, bf16[1,2048,896]{2,1,0:T(8,128)(2,1)}, u32[]{:S(2)}) copy-start(bf16[1,2048,896]{2,1,0:T(8,128)(2,1)} %param.19) | copy-start | bytes 11010052
  66.8 5.5 %copy-start.11 = (bf16[576,2048]{1,0:T(8,128)(2,1)S(1)}, bf16[576,2048]{1,0:T(8,128)(2,1)}, u32[]{:S(2)}) copy-start(bf16[576,2048]{1,0:T(8,128)(2,1)} %get-tuple-element.14) | copy-start | bytes 7077892
  72.3 2.7 %copy-start.17 = (f32[576,896]{1,0:T(8,128)}, f32[576,896]{1,0:T(8,128)S(1)}, u32[]{:S(2)}) copy-start(f32[576,896]{1,0:T(8,128)S(1)} %fusion.2) | copy-start | bytes 6193156
  72.3 2.8 %copy-start.8 = (bf16[1,896,2048]{2,1,0:T(8,128)(2,1)S(1)}, bf16[1,896,2048]{2,1,0:T(8,128)(2,1)}, u32[]{:S(2)}) copy-start(bf16[1,896,2048]{2,1,0:T(8,128)(2,1)} %param.20) | copy-start | bytes 11010052
  72.3 3.5 %copy-start.13 = (bf16[576,2048]{1,0:T(8,128)(2,1)S(1)}, bf16[576,2048]{1,0:T(8,128)(2,1)}, u32[]{:S(2)}) copy-start(bf16[576,2048]{1,0:T(8,128)(2,1)} %get-tuple-element.15) | copy-start | bytes 7077892
  75.0 4.1 %copy-start.19 = (f32[576,896]{1,0:T(8,128)}, f32[576,896]{1,0:T(8,128)S(1)}, u32[]{:S(2)}) copy-start(f32[576,896]{1,0:T(8,128)S(1)} %fusion.6) | copy-start | bytes 6193156
  75.8 4.2 %copy-start.9 = (bf16[1,2048,896]{2,1,0:T(8,128)(2,1)S(1)}, bf16[1,2048,896]{2,1,0:T(8,128)(2,1)}, u32[]{:S(2)}) copy-start(bf16[1,2048,896]{2,1,0:T(8,128)(2,1)} %param.18) | copy-start | bytes 11010052
  79.1 1.0 copy-start.15
  79.1 5.3 %copy-start.21 = (bf16[576,896]{1,0:T(8,128)(2,1)}, bf16[576,896]{1,0:T(8,128)(2,1)S(1)}, u32[]{:S(2)}) copy-start(bf16[576,896]{1,0:T(8,128)(2,1)S(1)} %get-tuple-element.22) | copy-start | bytes 3096580
  84.3 10.4 %copy-start.18 = (f32[576,896]{1,0:T(8,128)S(1)}, f32[576,896]{1,0:T(8,128)}, u32[]{:S(2)}) copy-start(f32[576,896]{1,0:T(8,128)} %copy-done.17) | copy-start | bytes 6193156
  84.3 10.4 %copy-start.20 = (f32[576,896]{1,0:T(8,128)S(1)}, f32[576,896]{1,0:T(8,128)}, u32[]{:S(2)}) copy-start(f32[576,896]{1,0:T(8,128)} %copy-done.19) | copy-start | bytes 6193156
  90.2 4.6 %copy-start.14 = (bf16[576,2048]{1,0:T(8,128)(2,1)S(1)}, bf16[576,2048]{1,0:T(8,128)(2,1)}, u32[]{:S(2)}) copy-start(bf16[576,2048]{1,0:T(8,128)(2,1)} %get-tuple-element.15) | copy-start | bytes 7077892
  91.1 8.5 %collective-permute-start = (bf16[288,512]{1,0:T(8,128)(2,1)}, bf16[288,512]{1,0:T(8,128)(2,1)S(1)}, u32[]{:S(2)}, u32[]{:S(2)}) collective-permute-start(bf16[288,512]{1,0:T(8,128)(2,1)} %get-tuple-element.26), channel_id=1, source_target_pairs={{0,1},{1,2},{2,3},{3,0},{4,5},{5,6},{6,7},{7,4},{8,9},{9,10},{10,1... | collective-permute-start | bytes 884744 | tf_op jit(solution)/shard_map/ppermute | solution.py:661
  91.2 16.0 %collective-permute-start.2 = (bf16[288,512]{1,0:T(8,128)(2,1)}, bf16[288,512]{1,0:T(8,128)(2,1)}, u32[]{:S(2)}, u32[]{:S(2)}) collective-permute-start(bf16[288,512]{1,0:T(8,128)(2,1)} %get-tuple-element.27), channel_id=1, source_target_pairs={{0,3},{1,0},{2,1},{3,2},{4,7},{5,4},{6,5},{7,6},{8,11},{9,8},{10,9... | collective-permute-start | bytes 884744 | tf_op jit(solution)/shard_map/ppermute | solution.py:664
  92.6 14.5 %collective-permute-start.4 = (bf16[288,512]{1,0:T(8,128)(2,1)}, bf16[288,512]{1,0:T(8,128)(2,1)}, u32[]{:S(2)}, u32[]{:S(2)}) collective-permute-start(bf16[288,512]{1,0:T(8,128)(2,1)} %get-tuple-element.28), channel_id=1, source_target_pairs={{0,3},{1,0},{2,1},{3,2},{4,7},{5,4},{6,5},{7,6},{8,11},{9,8},{10,9... | collective-permute-start | bytes 884744 | tf_op jit(solution)/shard_map/ppermute | solution.py:662
  94.8 4.7 %copy-start.7 = (s32[192,2]{0,1:T(2,128)S(1)}, s32[192,2]{0,1:T(2,128)}, u32[]{:S(2)}) copy-start(s32[192,2]{0,1:T(2,128)} %param.16) | copy-start | bytes 4612
  94.8 24.7 %collective-permute-start.3 = (bf16[288,512]{1,0:T(8,128)(2,1)S(1)}, bf16[288,512]{1,0:T(8,128)(2,1)S(1)}, u32[]{:S(2)}, u32[]{:S(2)}) collective-permute-start(bf16[288,512]{1,0:T(8,128)(2,1)S(1)} %get-tuple-element.29), channel_id=1, source_target_pairs={{0,1},{1,2},{2,3},{3,0},{4,5},{5,6},{6,7},{7,4},{8,9},{9,10},{10,1... | collective-permute-start | bytes 884744 | tf_op jit(solution)/shard_map/ppermute | solution.py:663
  99.7 14.9 %copy-start.12 = (bf16[576,2048]{1,0:T(8,128)(2,1)S(1)}, bf16[576,2048]{1,0:T(8,128)(2,1)}, u32[]{:S(2)}) copy-start(bf16[576,2048]{1,0:T(8,128)(2,1)} %get-tuple-element.14) | copy-start | bytes 7077892
  99.7 14.9 %copy-start.16 = (bf16[576,896]{1,0:T(8,128)(2,1)S(1)}, bf16[576,896]{1,0:T(8,128)(2,1)}, u32[]{:S(2)}) copy-start(bf16[576,896]{1,0:T(8,128)(2,1)} %copy-done.15) | copy-start | bytes 3096580
  99.7 10.4 %collective-permute-start.1 = (bf16[288,512]{1,0:T(8,128)(2,1)S(1)}, bf16[288,512]{1,0:T(8,128)(2,1)S(1)}, u32[]{:S(2)}, u32[]{:S(2)}) collective-permute-start(bf16[288,512]{1,0:T(8,128)(2,1)S(1)} %add_convert_fusion.4), channel_id=1, source_target_pairs={{0,1},{1,2},{2,3},{3,0},{4,5},{5,6},{6,7},{7,4},{8,9},{9,10},{10,1... | collective-permute-start | bytes 884744 | tf_op jit(solution)/shard_map/ppermute | solution.py:665
  111.4 8.1 %collective-permute-start.5 = (bf16[288,512]{1,0:T(8,128)(2,1)S(1)}, bf16[288,512]{1,0:T(8,128)(2,1)S(1)}, u32[]{:S(2)}, u32[]{:S(2)}) collective-permute-start(bf16[288,512]{1,0:T(8,128)(2,1)S(1)} %get-tuple-element.25), channel_id=1, source_target_pairs={{0,3},{1,0},{2,1},{3,2},{4,7},{5,4},{6,5},{7,6},{8,11},{9,8},{10,9... | collective-permute-start | bytes 884744 | tf_op jit(solution)/shard_map/ppermute | solution.py:666
  114.6 5.1 %copy-start.2 = (bf16[8,128,128]{2,1,0:T(8,128)(2,1)S(1)}, bf16[8,128,128]{2,1,0:T(8,128)(2,1)}, u32[]{:S(2)}) copy-start(bf16[8,128,128]{2,1,0:T(8,128)(2,1)} %wr_ref.3) | copy-start | bytes 786436
  114.6 5.1 %copy-start.3 = (bf16[8,128,128]{2,1,0:T(8,128)(2,1)S(1)}, bf16[8,128,128]{2,1,0:T(8,128)(2,1)}, u32[]{:S(2)}) copy-start(bf16[8,128,128]{2,1,0:T(8,128)(2,1)} %wi_ref.3) | copy-start | bytes 786436
  114.6 5.1 %copy-start.4 = (bf16[192,512]{1,0:T(8,128)(2,1)S(1)}, bf16[192,512]{1,0:T(8,128)(2,1)}, u32[]{:S(2)}) copy-start(bf16[192,512]{1,0:T(8,128)(2,1)} %og_ref.1) | copy-start | bytes 589828
  114.6 5.1 %copy-start.6 = (f32[32,2,256]{2,1,0:T(2,128)S(1)}, f32[32,2,256]{2,1,0:T(2,128)}, u32[]{:S(2)}) copy-start(f32[32,2,256]{2,1,0:T(2,128)} %get-tuple-element.18.gain_ref) | copy-start | bytes 196612
  119.5 1.3 copy-start
  119.5 1.6 copy-start.1
  119.5 1.6 copy-start.5
where the time goes:
time: 164 us; the launch traced here: 162 us
  Pallas kernels  105 us (64%)
  matrix products  38.2 us (23%)
  starting transfers between devices  6.88 us (4%)
  local copies, waits for them, and re-layouts  6.28 us (4%)
  waiting for transfers between devices  3.01 us (2%)
    pallas_call x1, Pallas kernels, dispatch(): pl.pallas_call(functools.partial(dispatch_kernel, n_sp), out_shape=(jax.S...  66.1 us
    pallas_call x1, Pallas kernels, tail(): pl.pallas_call(functools.partial(tail_kernel, n_sp), out_shape=(jax.Shape...  38.8 us
    dot_general x8, matrix products, mm(): lax.dot_general(a, b, (((ca,), (cb,)), ((), ())), preferred_element_type=...  38.2 us
    unnamed x48, local copies, waits for them, and re-layouts  5.32 us
  transfers between devices with their start and end apart: 6, of which 1 were waited for; matrix products, arithmetic and copies ran while one was open for 11% of the time, Pallas kernels for 0%

commit v1 on v0

--- a/solution.py
+++ b/solution.py
@@ -41,6 +41,16 @@
 
 def met(count):
     pl.semaphore_wait(pltpu.get_barrier_semaphore(), count)
+
+
+def in_blocks(body, total, size=256):
+    def step(n, c):
+        body(pl.multiple_of(n * size, size), size)
+        return c
+
+    lax.fori_loop(0, total // size, step, 0)
+    if total % size:
+        body(total - total % size, total % size)
 
 
 def shifted(value, by, fill, row):
@@ -93,16 +103,47 @@
     wi_ref,
     cdp_ref,
     eld_ref,
-    rows_ref,
-    cot_ref,
-    rec_ref,
-    lru_ref,
-    gain_ref,
+    wg_ref,
+    wu_ref,
+    wd_ref,
+    rows_out,
+    cot_out,
+    hid_out,
+    dg_out,
+    du_out,
+    own_out,
+    fwd_out,
+    bwd_out,
+    rec_out,
+    lru_out,
+    gain_out,
     send,
     recv,
     ext,
     stat,
     stats,
+    wg,
+    wu,
+    wd,
+    rows_ref,
+    cot_ref,
+    acc_g,
+    acc_u,
+    acc_d,
+    hid,
+    dg,
+    du,
+    far_out,
+    far_in,
+    own_sum,
+    fwd_sum,
+    bwd_sum,
+    rec_ref,
+    lru_ref,
+    w_sems,
+    out_sems,
+    f_send,
+    f_recv,
     d_send,
     d_recv,
     own_sem,
@@ -121,6 +162,12 @@
     extra = 2
     groups = 8
     per = n_sp // groups
+    loads = [
+        pltpu.make_async_copy(src.at[0], dst, w_sems.at[i])
+        for i, (src, dst) in enumerate(((wg_ref, wg), (wu_ref, wu), (wd_ref, wd)))
+    ]
+    for c in loads:
+        c.start()
     greet([(lax.rem(me + d, n_sp), tp) for d in range(1, n_sp)] + [(me, right), (me, left)])
 
     r0 = rt_ref[0:1, :].astype(F32)
@@ -191,7 +238,12 @@
         own_sem,
     )
     own.start()
-    sends = [dispatch(lax.rem(me + n_sp - d, n_sp), d) for d in range(1, n_sp)]
+    sends = []
+    for i in range(groups):
+        for k in range(per):
+            if i + k > 0:
+                to = lax.rem(me // per + groups - i, groups) * per + lax.rem(me + k, per)
+                sends.append(dispatch(to, i * per + k))
     for s in sends:
         s.start()
 
@@ -238,6 +290,32 @@
         )
 
     started = []
+    hidden = wg.shape[1]
+
+    def quarter(k, first):
+        cols = pl.ds(pl.multiple_of(k * feat, feat), feat)
+        rows_ref[0 : n_sp * MAIN, cols] = recv[k, :, 0:feat]
+        cot_ref[0 : n_sp * MAIN, cols] = recv[k, :, feat : 2 * feat]
+        ext[...] = recv[k, :, 2 * feat : 2 * feat + LANE].astype(F32)
+        for b in range(cuts):
+            at = pl.ds(pl.multiple_of(k * feat + b * LANE, LANE), LANE)
+            rows_ref[n_sp * MAIN :, at] = ext[pl.ds(b, n_sp * extra, stride=2 * cuts), :].astype(
+                BF16
+            )
+            cot_ref[n_sp * MAIN :, at] = ext[
+                pl.ds(cuts + b, n_sp * extra, stride=2 * cuts), :
+            ].astype(BF16)
+
+        def columns(at, size):
+            here = pl.ds(at, size)
+            for acc, made in (
+                (acc_g, lambda: mm(rows_ref[:, cols], wg[cols, here])),
+                (acc_u, lambda: mm(rows_ref[:, cols], wu[cols, here])),
+                (acc_d, lambda: mm(cot_ref[:, cols], wd[here, cols], 1, 1)),
+            ):
+                acc[:, here] = made() if first else acc[:, here] + made()
+
+        in_blocks(columns, hidden)
 
     def relay(i):
         if i % 2 == 0:
@@ -267,16 +345,18 @@
         ):
             c.start()
             started.append(c)
-        if i > 0:
-            relay(i - 1)
-
+
+    for c in loads:
+        c.wait()
+    quarter(tp, True)
+    for i in range(groups):
+        relay(i)
     for d in range(1, n_sp):
         source = lax.rem(me + d, n_sp)
         copy_to(stat.at[0], stats.at[source], s_send.at[0], s_recv.at[source], source, tp).wait_recv()
     carry = jnp.zeros((1, u.shape[1]), F32)
     for s in range(n_sp):
         carry = jnp.where(s < me, stats[s, 0:1, :] * carry + stats[s, 1:2, :], carry)
-    gain_ref[...] = stats[...]
     states = local + gain * carry
     row = lax.broadcasted_iota(jnp.int32, states.shape, 0)
     prev = jnp.where(row == 0, carry, pltpu.roll(states, 1, 0))
@@ -291,56 +371,139 @@
     )
     rec_ref[5] = uf * scale * admit * (1.0 - admit)
 
-    relay(groups - 1)
-    for i in range(groups):
-        if i % 2 == 1:
-            pass_on(left, i, l_send.at[i], fl_recv.at[i], right).wait_recv()
-        else:
-            pass_on(right, i, r_send.at[i], fr_recv.at[i], left).wait_recv()
+    for i in range(1, groups, 2):
+        pass_on(left, i, l_send.at[i], fl_recv.at[i], right).wait_recv()
+    quarter(left, False)
+    for i in range(0, groups, 2):
+        pass_on(right, i, r_send.at[i], fr_recv.at[i], left).wait_recv()
+    quarter(right, False)
     for i in range(groups):
         pass_on(far, i, y_send.at[i], ff_recv.at[i], right).wait_recv()
-
-    for q in range(4):
-        rows_ref[0 : n_sp * MAIN, q * feat : (q + 1) * feat] = recv[q, :, 0:feat]
-        cot_ref[0 : n_sp * MAIN, q * feat : (q + 1) * feat] = recv[q, :, feat : 2 * feat]
-        ext[...] = recv[q, :, 2 * feat : 2 * feat + LANE].astype(F32)
-        for b in range(cuts):
-            at = q * feat + b * LANE
-            rows_ref[n_sp * MAIN :, at : at + LANE] = ext[
-                pl.ds(b, n_sp * extra, stride=2 * cuts), :
-            ].astype(BF16)
-            cot_ref[n_sp * MAIN :, at : at + LANE] = ext[
-                pl.ds(cuts + b, n_sp * extra, stride=2 * cuts), :
-            ].astype(BF16)
-
+    quarter(far, False)
+    outs = []
+
+    def put(src, dst):
+        outs.append(pltpu.make_async_copy(src, dst, out_sems.at[len(outs)]))
+        outs[-1].start()
+
+    put(rows_ref, rows_out)
+    put(cot_ref, cot_out)
+    put(rec_ref, rec_out)
+    put(lru_ref, lru_out)
+    put(stats, gain_out)
+    strip = 32
+
+    def activate(i, c):
+        at = pl.ds(pl.multiple_of(i * strip, strip), strip)
+        gate = acc_g[at, :]
+        up = acc_u[at, :]
+        d_hidden = acc_d[at, :]
+        sig = jax.nn.sigmoid(gate)
+        silu = gate * sig
+        hid[at, :] = (silu * up).astype(BF16)
+        dg[at, :] = (d_hidden * up * sig * (1.0 + gate * (1.0 - sig))).astype(BF16)
+        du[at, :] = (d_hidden * silu).astype(BF16)
+        return c
+
+    slots = rows_ref.shape[0]
+    lax.fori_loop(0, slots // strip, activate, 0)
+    put(hid, hid_out)
+    put(dg, dg_out)
+    put(du, du_out)
+
+    def back_to(k, store):
+        def columns(at, size):
+            here = pl.ds(pl.multiple_of(k * feat + at, LANE), size)
+            store(at, size, mm(dg[...], wg[here, :], 1, 1) + mm(du[...], wu[here, :], 1, 1))
+
+        in_blocks(columns, feat)
+
+    def into(ref, kind):
+        def store(at, size, value):
+            ref[:, pl.ds(at, size)] = value.astype(kind)
+
+        return store
+
+    half = slots // 2
+    back_to(far, into(far_out, BF16))
+    top, low = pl.ds(0, half), pl.ds(half, half)
+    for n, (rows, to) in enumerate(((top, right), (low, left))):
+        c = copy_to(far_out.at[rows], far_in.at[rows], f_send.at[n], f_recv.at[n], me, to)
+        c.start()
+        started.append(c)
+    back_to(tp, into(own_sum, BF16))
+    put(own_sum, own_out)
+    back_to(right, into(acc_g, F32))
+    back_to(left, into(acc_u, F32))
+    fwd_sum[half:, :] = acc_g[half:, 0:feat].astype(BF16)
+    bwd_sum[0:half, :] = acc_u[0:half, 0:feat].astype(BF16)
+    for c in started[-2:]:
+        c.wait_recv()
+    fwd_sum[0:half, :] = (acc_g[0:half, 0:feat] + far_in[0:half, :].astype(F32)).astype(BF16)
+    bwd_sum[half:, :] = (acc_u[half:, 0:feat] + far_in[half:, :].astype(F32)).astype(BF16)
+    put(fwd_sum, fwd_out)
+    put(bwd_sum, bwd_out)
+    for c in outs:
+        c.wait()
     for c in sends + told + started:
         c.wait_send()
 
 
-def dispatch(n_sp, x, g, rt, wt, u, ogl, wr, wi, cdp, eld):
+def dispatch(n_sp, x, g, rt, wt, u, ogl, wr, wi, cdp, eld, wg, wu, wd):
     tokens, feat = x.shape
     chans = u.shape[1]
     slots = n_sp * (MAIN + 2)
     width = 2 * feat + LANE
+    hidden = wg.shape[2]
+    shape = jax.ShapeDtypeStruct
+    anywhere = pl.BlockSpec(memory_space=pl.ANY)
     vmem = pl.BlockSpec(memory_space=pltpu.VMEM)
     dma = pltpu.SemaphoreType.DMA
     return pl.pallas_call(
         functools.partial(dispatch_kernel, n_sp),
         out_shape=(
-            jax.ShapeDtypeStruct((slots, 4 * feat), BF16),
-            jax.ShapeDtypeStruct((slots, 4 * feat), BF16),
-            jax.ShapeDtypeStruct((6, tokens, chans), F32),
-            jax.ShapeDtypeStruct((tokens, chans), BF16),
-            jax.ShapeDtypeStruct((n_sp, 2, chans), F32),
+            shape((slots, 4 * feat), BF16),
+            shape((slots, 4 * feat), BF16),
+            shape((slots, hidden), BF16),
+            shape((slots, hidden), BF16),
+            shape((slots, hidden), BF16),
+            shape((slots, feat), BF16),
+            shape((slots, feat), BF16),
+            shape((slots, feat), BF16),
+            shape((6, tokens, chans), F32),
+            shape((tokens, chans), BF16),
+            shape((n_sp, 2, chans), F32),
         ),
-        in_specs=[vmem] * 10,
-        out_specs=(vmem,) * 5,
+        in_specs=[vmem] * 10 + [anywhere] * 3,
+        out_specs=(anywhere,) * 11,
         scratch_shapes=[
             pltpu.VMEM((n_sp * MAIN, width), BF16),
             pltpu.VMEM((4, n_sp * MAIN, width), BF16),
             pltpu.VMEM((n_sp * MAIN, LANE), F32),
             pltpu.VMEM((1, 2, chans), F32),
             pltpu.VMEM((n_sp, 2, chans), F32),
+            pltpu.VMEM((4 * feat, hidden), BF16),
+            pltpu.VMEM((4 * feat, hidden), BF16),
+            pltpu.VMEM((hidden, 4 * feat), BF16),
+            pltpu.VMEM((slots, 4 * feat), BF16),
+            pltpu.VMEM((slots, 4 * feat), BF16),
+            pltpu.VMEM((slots, hidden), F32),
+            pltpu.VMEM((slots, hidden), F32),
+            pltpu.VMEM((slots, hidden), F32),
+            pltpu.VMEM((slots, hidden), BF16),
+            pltpu.VMEM((slots, hidden), BF16),
+            pltpu.VMEM((slots, hidden), BF16),
+            pltpu.VMEM((slots, feat), BF16),
+            pltpu.VMEM((slots, feat), BF16),
+            pltpu.VMEM((slots, feat), BF16),
+            pltpu.VMEM((slots, feat), BF16),
+            pltpu.VMEM((slots, feat), BF16),
+            pltpu.VMEM((6, tokens, chans), F32),
+            pltpu.VMEM((tokens, chans), BF16),
+            dma((3,)),
+            dma((11,)),
+            dma((2,)),
+            dma((2,)),
             dma((n_sp,)),
             dma((n_sp,)),
             dma,
@@ -357,12 +520,14 @@
             collective_id=0, has_side_effects=True, vmem_limit_bytes=60 * 1024 * 1024
         ),
         name="dispatch",
-    )(x, g, rt, wt, u, ogl, wr, wi, cdp, eld)
+    )(x, g, rt, wt, u, ogl, wr, wi, cdp, eld, wg, wu, wd)
 
 
 def tail_kernel(
     n_sp,
-    sg_ref,
+    own_ref,
+    fwd_ref,
+    bwd_ref,
     og_ref,
     routes_ref,
     wout_ref,
@@ -374,6 +539,7 @@
     gop_ref,
     gin_ref,
     ggp_ref,
+    sg_ref,
     rext,
     arr,
     arrx,
@@ -412,6 +578,9 @@
     greet([(lax.rem(me + d, n_sp), tp) for d in range(1, n_sp)] + [(me, right), (me, left)])
 
     main = n_sp * MAIN
+    sg_ref[...] = (
+        own_ref[...].astype(F32) + (fwd_ref[...].astype(F32) + bwd_ref[...].astype(F32))
+    ).astype(BF16)
     sx = sg_ref[main:, :].astype(F32)
     for b in range(cuts):
         rext[pl.ds(b, n_sp * extra, stride=cuts), :] = sx[:, b * LANE : (b + 1) * LANE]
@@ -603,7 +772,7 @@
         c.wait_send()
 
 
-def tail(n_sp, sg, og, routes, wout, wr, wi, rec, lru, gains):
+def tail(n_sp, own, fwd, bwd, og, routes, wout, wr, wi, rec, lru, gains):
     tokens, feat = og.shape
     chans = lru.shape[1]
     chips = n_sp // 2
@@ -618,9 +787,10 @@
             jax.ShapeDtypeStruct((tokens, chans), F32),
             jax.ShapeDtypeStruct((tokens, chans), F32),
         ),
-        in_specs=[vmem] * 9,
+        in_specs=[vmem] * 11,
         out_specs=(vmem,) * 3,
         scratch_shapes=[
+            pltpu.VMEM(own.shape, BF16),
             pltpu.VMEM((n_sp * xrows, LANE), F32),
             pltpu.VMEM((n_sp * MAIN, feat), BF16),
             pltpu.VMEM((n_sp * xrows, LANE), F32),
@@ -650,23 +820,7 @@
             collective_id=1, has_side_effects=True, vmem_limit_bytes=40 * 1024 * 1024
         ),
         name="tail",
-    )(sg, og, routes, wout, wr, wi, rec, lru, gains)
-
-
-def summed_over_tp(parts):
-    fwd = [(k, (k + 1) % 4) for k in range(4)]
-    bwd = [(k, (k + 3) % 4) for k in range(4)]
-    here, right, far, left = parts
-    half = here.shape[0] // 2
-    far_a = lax.ppermute(far[:half], "tp", fwd)
-    far_b = lax.ppermute(far[half:], "tp", bwd)
-    right_b = lax.ppermute(right[half:], "tp", fwd)
-    left_a = lax.ppermute(left[:half], "tp", bwd)
-    right_a = lax.ppermute((right[:half].astype(F32) + far_a.astype(F32)).astype(BF16), "tp", fwd)
-    left_b = lax.ppermute((left[half:].astype(F32) + far_b.astype(F32)).astype(BF16), "tp", bwd)
-    top = here[:half].astype(F32) + (right_a.astype(F32) + left_a.astype(F32))
-    low = here[half:].astype(F32) + (right_b.astype(F32) + left_b.astype(F32))
-    return jnp.concatenate([top, low], axis=0).astype(BF16)
+    )(own, fwd, bwd, og, routes, wout, wr, wi, rec, lru, gains)
 
 
 def per_device(
@@ -686,8 +840,7 @@
     channel_decay_param,
     extra_log_decay,
 ):
-    feat = middle_stream.shape[1]
-    inputs, cotangent, rec, lru, gains = dispatch(
+    inputs, cotangent, hidden, d_gate, d_up, own, fwd, bwd, rec, lru, gains = dispatch(
         n_sp,
         middle_stream,
         output_gradient,
@@ -699,34 +852,20 @@
         input_gate_weight,
         channel_decay_param[None],
         extra_log_decay,
+        expert_gate_weight,
+        expert_up_weight,
+        expert_down_weight,
     )
-    gate_weight, up_weight, down_weight = (
-        expert_gate_weight[0],
-        expert_up_weight[0],
-        expert_down_weight[0],
-    )
-    gate_act = mm(inputs, gate_weight)
-    up_act = mm(inputs, up_weight)
-    sigmoid_gate = jax.nn.sigmoid(gate_act)
-    silu_act = gate_act * sigmoid_gate
-    hidden = (silu_act * up_act).astype(BF16)
-    d_hidden = mm(cotangent, down_weight, 1, 1)
-    d_gate = (d_hidden * up_act * sigmoid_gate * (1.0 + gate_act * (1.0 - sigmoid_gate))).astype(
-        BF16
-    )
-    d_up = (d_hidden * silu_act).astype(BF16)
-    partial = (mm(d_gate, gate_weight, 1, 1) + mm(d_up, up_weight, 1, 1)).astype(BF16)
-    tp = lax.axis_index("tp")
-    parts = [
-        lax.dynamic_slice_in_dim(partial, lax.rem(tp + k, 4) * feat, feat, 1) for k in range(4)
-    ]
-    slot_grad = summed_over_tp(parts)
+    fwd = lax.ppermute(fwd, "tp", [(k, (k + 1) % 4) for k in range(4)])
+    bwd = lax.ppermute(bwd, "tp", [(k, (k + 3) % 4) for k in range(4)])
     grad_down = mm(hidden, cotangent, 0, 0).astype(BF16)
     grad_gate = mm(inputs, d_gate, 0, 0).astype(BF16)
     grad_up = mm(inputs, d_up, 0, 0).astype(BF16)
     grad_out_proj, grad_input, grad_gate_pre = tail(
         n_sp,
-        slot_grad,
+        own,
+        fwd,
+        bwd,
         output_gradient,
         routes,
         recurrent_output_weight,

time: 164 us -> 134 us (0.82)
  matrix products: 38.2 us -> 18.8 us
  starting transfers between devices: 6.88 us -> 1.53 us
  local copies, waits for them, and re-layouts: 6.28 us -> 2.16 us
  Pallas kernels: 105 us -> 108 us
  waiting for transfers between devices: 3.01 us -> 0.01 us
    dot_general x8 -> x3, matrix products: 38.2 us -> 18.8 us  [mm(): lax.dot_general(a, b, (((ca,), (cb,)), ((), ())), preferred_element_type=...]
    ppermute x6 -> x2, starting transfers between devices: 6.88 us -> 1.53 us  [the longest x1 1.45 us: per_device(): bwd = lax.ppermute(bwd, 'tp', [(k, (k + 3) % 4) for k in range(4)])]
    unnamed x48 -> x28, local copies, waits for them, and re-layouts: 5.32 us -> 2.16 us
    ppermute x6 -> x2, waiting for transfers between devices: 3.01 us -> 0.01 us  [the longest x1 0.01 us: per_device(): fwd = lax.ppermute(fwd, 'tp', [(k, (k + 1) % 4) for k in range(4)])]
    pallas_call x1, Pallas kernels: 38.8 us -> 40.5 us  [tail(): pl.pallas_call(functools.partial(tail_kernel, n_sp), out_shape=(jax.Shape...]
  transfers between devices with their start and end apart: 6 -> 2, of which waited for: 1 -> 0; matrix products, arithmetic and copies ran while one was open for 11% -> 14% of each run, Pallas kernels for 0% -> 0%
where the time goes in v1:
time: 134 us; the launch traced here: 131 us
  Pallas kernels  108 us (81%)
  matrix products  18.8 us (14%)
  local copies, waits for them, and re-layouts  2.16 us (2%)
  starting transfers between devices  1.53 us (1%)
    pallas_call x1, Pallas kernels, dispatch(): pl.pallas_call(functools.partial(dispatch_kernel, n_sp), out_shape=(shape...  67.7 us
    pallas_call x1, Pallas kernels, tail(): pl.pallas_call(functools.partial(tail_kernel, n_sp), out_shape=(jax.Shape...  40.5 us
    dot_general x3, matrix products, mm(): lax.dot_general(a, b, (((ca,), (cb,)), ((), ())), preferred_element_type=...  18.8 us
  transfers between devices with their start and end apart: 2, of which 0 were waited for; matrix products, arithmetic and copies ran while one was open for 14% of the time, Pallas kernels for 0%

profile of v1, /device:TPU:27, one launch (start us, length us, event | category | flops | bytes accessed | tf_op | source)
XLA Modules:
  0.0 131.5 jit_solution(5691020349268443273)
XLA Ops:
  0.6 67.7 %dispatch.1 = (bf16[576,2048]{1,0:T(8,128)(2,1)}, bf16[576,2048]{1,0:T(8,128)(2,1)}, bf16[576,896]{1,0:T(8,128)(2,1)}, bf16[576,896]{1,0:T(8,128)(2,1)}, bf16[57...) custom-call(bf16[192,512]{1,0:T(8,128)(2,1)} %x_ref.1, ...), custom_call_target="tpu_custom_call" | custom-call | tf_op jit(solution)/shard_map/dispatch/pallas_call | solution.py:462
  68.3 0.1 collective-permute-start
  68.4 1.5 %collective-permute-start.1 = (bf16[576,512]{1,0:T(8,128)(2,1)}, bf16[576,512]{1,0:T(8,128)(2,1)S(1)}, u32[]{:S(2)}, u32[]{:S(2)}) collective-permute-start(bf16[576,512]{1,0:T(8,128)(2,1)} %get-tuple-element.27), channel_id=1, source_target_pairs={{0,3},{1,0},{2,1},{3,2},{4,7},{5,4},{6,5},{7,6},{8,11},{9,8},{10,9... | collective-permute-start | bytes 1769480 | tf_op jit(solution)/shard_map/ppermute | solution.py:860
  69.8 7.3 %convert_bitcast_fusion.2 = bf16[1,2048,896]{2,1,0:T(8,128)(2,1)} fusion(bf16[576,2048]{1,0:T(8,128)(2,1)} %get-tuple-element.20, bf16[576,896]{1,0:T(8,128)(2,1)} %get-tuple-element.21), kind=kOutput, calls=%fused_computation.2 | convolution fusion | flops 2115764224 | bytes 7061504 | tf_op jit(solution)/shard_map/dot_general | solution.py:18
  77.1 0.0 copy-done.9
  77.1 0.0 copy-done.11
  77.1 0.0 copy-start.10
  77.1 4.8 %convert_bitcast_fusion.1 = bf16[1,2048,896]{2,1,0:T(8,128)(2,1)} fusion(bf16[576,2048]{1,0:T(8,128)(2,1)S(1)} %copy-done.9, bf16[576,896]{1,0:T(8,128)(2,1)S(1)} %copy-done.11), kind=kOutput, calls=%fused_computation.1 | convolution fusion | flops 2115764224 | bytes 7061504 | tf_op jit(solution)/shard_map/dot_general | solution.py:18
  82.0 0.0 copy-done.8
  82.0 0.1 copy.20.routes_ref
  82.1 0.0 copy-done.10
  82.1 0.0 copy-start
  82.1 0.0 copy-start.1
  82.1 0.0 copy-start.2
  82.2 0.0 copy-start.3
  82.2 0.0 copy-start.4
  82.2 0.0 copy-start.5
  82.2 0.0 copy-start.6
  82.2 0.0 copy-start.7
  82.2 6.7 %convert_bitcast_fusion = bf16[1,896,2048]{2,1,0:T(8,128)(2,1)} fusion(bf16[576,896]{1,0:T(8,128)(2,1)S(1)} %copy-done.10, bf16[576,2048]{1,0:T(8,128)(2,1)} %get-tuple-element.24), kind=kOutput, calls=%fused_computation | convolution fusion | flops 2115764224 | bytes 7061504 | tf_op jit(solution)/shard_map/dot_general | solution.py:18
  88.9 0.0 collective-permute-done.fwd_ref
  88.9 0.0 collective-permute-done.1.bwd_ref
  88.9 0.0 copy-done
  88.9 0.0 copy-done.1
  89.0 0.0 copy-done.2
  89.0 0.0 copy-done.3
  89.0 0.0 copy-done.4
  89.0 0.0 copy-done.5
  89.0 40.5 %tail.1 = (f32[64,256]{1,0:T(8,128)S(1)}, f32[192,256]{1,0:T(8,128)S(1)}, f32[192,256]{1,0:T(8,128)S(1)}) custom-call(bf16[576,512]{1,0:T(8,128)(2,1)S(1)} %copy-done.5, bf16[576,512]{1,0:T(8,128)(2,1)S(1)} %collective-permute-done.fwd_ref, bf16[576,512]{1,0:T(8,128)(2,1)S(1)} %collective-permute-done.1.bwd_ref, bf16[192,512]{1,0:T(8,128)(2,1)S(1)} %copy-done.4, ...), custom_call_target="tpu_custom_call" | custom-call | tf_op jit(solution)/shard_map/tail/pallas_call | solution.py:783
  129.5 0.6 copy.24
  130.1 0.7 copy.25
  130.8 0.7 copy.26
  (5 shorter events, 0.0 us)
Async XLA Ops:
  68.3 20.6 %collective-permute-start = (bf16[576,512]{1,0:T(8,128)(2,1)}, bf16[576,512]{1,0:T(8,128)(2,1)S(1)}, u32[]{:S(2)}, u32[]{:S(2)}) collective-permute-start(bf16[576,512]{1,0:T(8,128)(2,1)} %get-tuple-element.26), channel_id=1, source_target_pairs={{0,1},{1,2},{2,3},{3,0},{4,5},{5,6},{6,7},{7,4},{8,9},{9,10},{10,1... | collective-permute-start | bytes 1769480 | tf_op jit(solution)/shard_map/ppermute | solution.py:859
  68.4 20.6 %collective-permute-start.1 = (bf16[576,512]{1,0:T(8,128)(2,1)}, bf16[576,512]{1,0:T(8,128)(2,1)S(1)}, u32[]{:S(2)}, u32[]{:S(2)}) collective-permute-start(bf16[576,512]{1,0:T(8,128)(2,1)} %get-tuple-element.27), channel_id=1, source_target_pairs={{0,3},{1,0},{2,1},{3,2},{4,7},{5,4},{6,5},{7,6},{8,11},{9,8},{10,9... | collective-permute-start | bytes 1769480 | tf_op jit(solution)/shard_map/ppermute | solution.py:860
  69.8 7.3 %copy-start.9 = (bf16[576,2048]{1,0:T(8,128)(2,1)S(1)}, bf16[576,2048]{1,0:T(8,128)(2,1)}, u32[]{:S(2)}) copy-start(bf16[576,2048]{1,0:T(8,128)(2,1)} %get-tuple-element.20) | copy-start | bytes 7077892
  69.8 7.3 %copy-start.11 = (bf16[576,896]{1,0:T(8,128)(2,1)S(1)}, bf16[576,896]{1,0:T(8,128)(2,1)}, u32[]{:S(2)}) copy-start(bf16[576,896]{1,0:T(8,128)(2,1)} %get-tuple-element.22) | copy-start | bytes 3096580
  77.1 4.9 %copy-start.8 = (s32[192,2]{0,1:T(2,128)S(1)}, s32[192,2]{0,1:T(2,128)}, u32[]{:S(2)}) copy-start(s32[192,2]{0,1:T(2,128)} %param.16) | copy-start | bytes 4612
  77.1 5.0 %copy-start.10 = (bf16[576,896]{1,0:T(8,128)(2,1)S(1)}, bf16[576,896]{1,0:T(8,128)(2,1)}, u32[]{:S(2)}) copy-start(bf16[576,896]{1,0:T(8,128)(2,1)} %get-tuple-element.23) | copy-start | bytes 3096580
  82.1 6.8 %copy-start = (f32[6,192,256]{2,1,0:T(8,128)S(1)}, f32[6,192,256]{2,1,0:T(8,128)}, u32[]{:S(2)}) copy-start(f32[6,192,256]{2,1,0:T(8,128)} %get-tuple-element.28.rec_ref) | copy-start | bytes 3538948
  82.1 6.8 %copy-start.1 = (bf16[2048,256]{1,0:T(8,128)(2,1)S(1)}, bf16[2048,256]{1,0:T(8,128)(2,1)}, u32[]{:S(2)}) copy-start(bf16[2048,256]{1,0:T(8,128)(2,1)} %wout_ref.1) | copy-start | bytes 3145732
  82.1 6.8 %copy-start.2 = (bf16[8,128,128]{2,1,0:T(8,128)(2,1)S(1)}, bf16[8,128,128]{2,1,0:T(8,128)(2,1)}, u32[]{:S(2)}) copy-start(bf16[8,128,128]{2,1,0:T(8,128)(2,1)} %wr_ref.3) | copy-start | bytes 786436
  82.2 6.8 %copy-start.3 = (bf16[8,128,128]{2,1,0:T(8,128)(2,1)S(1)}, bf16[8,128,128]{2,1,0:T(8,128)(2,1)}, u32[]{:S(2)}) copy-start(bf16[8,128,128]{2,1,0:T(8,128)(2,1)} %wi_ref.3) | copy-start | bytes 786436
  82.2 6.8 %copy-start.4 = (bf16[192,512]{1,0:T(8,128)(2,1)S(1)}, bf16[192,512]{1,0:T(8,128)(2,1)}, u32[]{:S(2)}) copy-start(bf16[192,512]{1,0:T(8,128)(2,1)} %og_ref.1) | copy-start | bytes 589828
  82.2 6.8 %copy-start.5 = (bf16[576,512]{1,0:T(8,128)(2,1)S(1)}, bf16[576,512]{1,0:T(8,128)(2,1)}, u32[]{:S(2)}) copy-start(bf16[576,512]{1,0:T(8,128)(2,1)} %get-tuple-element.25.own_ref) | copy-start | bytes 1769476
  82.2 6.8 %copy-start.6 = (bf16[192,256]{1,0:T(8,128)(2,1)S(1)}, bf16[192,256]{1,0:T(8,128)(2,1)}, u32[]{:S(2)}) copy-start(bf16[192,256]{1,0:T(8,128)(2,1)} %get-tuple-element.29.lru_ref) | copy-start | bytes 294916
  82.2 6.8 %copy-start.7 = (f32[32,2,256]{2,1,0:T(2,128)S(1)}, f32[32,2,256]{2,1,0:T(2,128)}, u32[]{:S(2)}) copy-start(f32[32,2,256]{2,1,0:T(2,128)} %get-tuple-element.30.gain_ref) | copy-start | bytes 196612

commit v2 on v1

--- a/solution.py
+++ b/solution.py
@@ -119,6 +119,15 @@
     gain_out,
     send,
     recv,
+    picked,
+    pre_in,
+    x_far,
+    send_far,
+    recv_far,
+    pre_send,
+    pre_recv,
+    h_send,
+    h_recv,
     ext,
     stat,
     stats,
@@ -135,6 +144,8 @@
     du,
     far_out,
     far_in,
+    right_dx,
+    left_dx,
     own_sum,
     fwd_sum,
     bwd_sum,
@@ -195,6 +206,7 @@
         p1 = slot == m1
         pick = (p0 | p1).astype(F32).astype(BF16)
         weight = jnp.sum(jnp.where(p0, w0, 0.0) + jnp.where(p1, w1, 0.0), axis=1, keepdims=True)
+        picked[at : at + block, :] = pick
         send[at : at + block, 0:feat] = mm(pick, x).astype(BF16)
         send[at : at + block, feat : 2 * feat] = (mm(pick, g) * weight).astype(BF16)
     slot = iota((n_sp * extra, tokens), 0)
@@ -238,12 +250,34 @@
         own_sem,
     )
     own.start()
+    own_half = me // (n_sp // 2)
+    quad = groups // 2
+    g0 = me // per
+    mid = tokens // 2
+
+    def ahead(n, src, dst, to):
+        return copy_to(src, dst, pre_send.at[n], pre_recv.at[n], me, to)
+
+    first_hop = [
+        ahead(0, x_ref.at[pl.ds(0, mid)], pre_in.at[0], right),
+        ahead(1, x_ref.at[pl.ds(mid, mid)], pre_in.at[1], left),
+    ]
+    next_hop = [
+        ahead(2, pre_in.at[0], x_far.at[pl.ds(0, mid)], right),
+        ahead(3, pre_in.at[1], x_far.at[pl.ds(mid, mid)], left),
+    ]
+    for c in first_hop:
+        c.start()
+
+    def taker(i, k):
+        group = lax.rem(own_half + i // quad, 2) * quad + lax.rem(g0 + groups - i, quad)
+        return group * per + lax.rem(me + k, per)
+
     sends = []
     for i in range(groups):
         for k in range(per):
             if i + k > 0:
-                to = lax.rem(me // per + groups - i, groups) * per + lax.rem(me + k, per)
-                sends.append(dispatch(to, i * per + k))
+                sends.append(dispatch(taker(i, k), i * per + k))
     for s in sends:
         s.start()
 
@@ -278,60 +312,110 @@
         s.start()
 
     size = per * MAIN
-    g0 = me // per
+
+    def group_of(i):
+        return lax.rem(own_half + i // quad, 2) * quad + lax.rem(g0 + i, quad)
 
     def span(i):
-        start = lax.rem(g0 + i, groups) * size
-        return pl.ds(pl.multiple_of(start, size), size)
+        return pl.ds(pl.multiple_of(group_of(i) * size, size), size)
 
     def pass_on(quarter, i, send_sem, recv_sem, to):
         return copy_to(
             recv.at[quarter, span(i)], recv.at[quarter, span(i)], send_sem, recv_sem, me, to
         )
 
+    def pass_far(quarter, i, to):
+        part = recv.at[quarter, span(i), pl.ds(feat, feat + LANE)]
+        return copy_to(part, part, y_send.at[i], ff_recv.at[i], me, to)
+
+    def hand_over(peer, sem):
+        return copy_to(
+            send_far.at[pl.ds(pl.multiple_of(peer * MAIN, MAIN), MAIN)],
+            recv_far.at[pl.ds(pl.multiple_of(me * MAIN, MAIN), MAIN)],
+            h_send.at[sem],
+            h_recv.at[me],
+            peer,
+            tp,
+        )
+
+    def handed(source):
+        part = recv_far.at[pl.ds(pl.multiple_of(source * MAIN, MAIN), MAIN)]
+        return copy_to(part, part, h_send.at[0], h_recv.at[source], source, tp)
+
     started = []
     hidden = wg.shape[1]
 
-    def quarter(k, first):
+    main = n_sp * MAIN
+    wide = main // 2
+
+    def from_half(h):
+        return pl.ds(pl.multiple_of(lax.rem(own_half + h, 2) * wide, wide), wide)
+
+    def place(k, x_from, halves, with_extra):
         cols = pl.ds(pl.multiple_of(k * feat, feat), feat)
-        rows_ref[0 : n_sp * MAIN, cols] = recv[k, :, 0:feat]
-        cot_ref[0 : n_sp * MAIN, cols] = recv[k, :, feat : 2 * feat]
-        ext[...] = recv[k, :, 2 * feat : 2 * feat + LANE].astype(F32)
-        for b in range(cuts):
-            at = pl.ds(pl.multiple_of(k * feat + b * LANE, LANE), LANE)
-            rows_ref[n_sp * MAIN :, at] = ext[pl.ds(b, n_sp * extra, stride=2 * cuts), :].astype(
-                BF16
-            )
-            cot_ref[n_sp * MAIN :, at] = ext[
-                pl.ds(cuts + b, n_sp * extra, stride=2 * cuts), :
-            ].astype(BF16)
+        for h in halves:
+            rows_ref[h * wide : (h + 1) * wide, cols] = x_from(from_half(h))
+            cot_ref[h * wide : (h + 1) * wide, cols] = recv[k, from_half(h), feat : 2 * feat]
+        if with_extra:
+            ext[...] = recv[k, :, 2 * feat : 2 * feat + LANE].astype(F32)
+            for b in range(cuts):
+                at = pl.ds(pl.multiple_of(k * feat + b * LANE, LANE), LANE)
+                rows_ref[main:, at] = ext[pl.ds(b, n_sp * extra, stride=2 * cuts), :].astype(BF16)
+                cot_ref[main:, at] = ext[
+                    pl.ds(cuts + b, n_sp * extra, stride=2 * cuts), :
+                ].astype(BF16)
+
+    def contract(k, lo, hi, first):
+        cols = pl.ds(pl.multiple_of(k * feat, feat), feat)
 
         def columns(at, size):
             here = pl.ds(at, size)
             for acc, made in (
-                (acc_g, lambda: mm(rows_ref[:, cols], wg[cols, here])),
-                (acc_u, lambda: mm(rows_ref[:, cols], wu[cols, here])),
-                (acc_d, lambda: mm(cot_ref[:, cols], wd[here, cols], 1, 1)),
+                (acc_g, lambda: mm(rows_ref[lo:hi, cols], wg[cols, here])),
+                (acc_u, lambda: mm(rows_ref[lo:hi, cols], wu[cols, here])),
+                (acc_d, lambda: mm(cot_ref[lo:hi, cols], wd[here, cols], 1, 1)),
             ):
-                acc[:, here] = made() if first else acc[:, here] + made()
+                acc[lo:hi, here] = made() if first else acc[lo:hi, here] + made()
 
         in_blocks(columns, hidden)
+
+    def near_half(k, h, odd, sent, arrived, to):
+        for i in range(h * quad + odd, (h + 1) * quad, 2):
+            pass_on(k, i, sent.at[i], arrived.at[i], to).wait_recv()
+        place(k, lambda rows: recv[k, rows, 0:feat], (h,), h == 1)
+        contract(k, h * wide, main + n_sp * extra if h else wide, False)
 
     def relay(i):
         if i % 2 == 0:
             pass_on(left, i, l_send.at[i], fl_recv.at[i], right).wait_recv()
-            c = pass_on(left, i, y_send.at[i], ff_recv.at[i], right)
+            c = pass_far(left, i, right)
         else:
             pass_on(right, i, r_send.at[i], fr_recv.at[i], left).wait_recv()
-            c = pass_on(right, i, y_send.at[i], ff_recv.at[i], left)
+            c = pass_far(right, i, left)
         c.start()
         started.append(c)
 
+    for c, n in zip(first_hop, next_hop):
+        c.wait_recv()
+        n.start()
     for i in range(groups):
         if i == 0:
             own.wait()
+        if i == 3:
+            for c in next_hop:
+                c.wait_recv()
+            for at in range(0, main, block):
+                send_far[at : at + block, :] = mm(picked[at : at + block, :], x_far[...]).astype(
+                    BF16
+                )
+            kept = pl.ds(pl.multiple_of(me * MAIN, MAIN), MAIN)
+            recv_far[kept, :] = send_far[kept, :]
+            for n in range(1, n_sp):
+                c = hand_over(taker(n // per, n % per), n)
+                c.start()
+                started.append(c)
         for k in range(per):
-            source = lax.rem(g0 + i, groups) * per + k
+            source = group_of(i) * per + k
             if i == 0:
 
                 @pl.when(source != me)
@@ -345,12 +429,16 @@
         ):
             c.start()
             started.append(c)
+        if i == quad - 1:
+            for n in range(quad):
+                relay(n)
 
     for c in loads:
         c.wait()
-    quarter(tp, True)
-    for i in range(groups):
-        relay(i)
+    place(tp, lambda rows: recv[tp, rows, 0:feat], (0, 1), True)
+    contract(tp, 0, main + n_sp * extra, True)
+    near_half(left, 0, 1, l_send, fl_recv, right)
+    near_half(right, 0, 0, r_send, fr_recv, left)
     for d in range(1, n_sp):
         source = lax.rem(me + d, n_sp)
         copy_to(stat.at[0], stats.at[source], s_send.at[0], s_recv.at[source], source, tp).wait_recv()
@@ -371,26 +459,12 @@
     )
     rec_ref[5] = uf * scale * admit * (1.0 - admit)
 
-    for i in range(1, groups, 2):
-        pass_on(left, i, l_send.at[i], fl_recv.at[i], right).wait_recv()
-    quarter(left, False)
-    for i in range(0, groups, 2):
-        pass_on(right, i, r_send.at[i], fr_recv.at[i], left).wait_recv()
-    quarter(right, False)
-    for i in range(groups):
-        pass_on(far, i, y_send.at[i], ff_recv.at[i], right).wait_recv()
-    quarter(far, False)
     outs = []
 
     def put(src, dst):
         outs.append(pltpu.make_async_copy(src, dst, out_sems.at[len(outs)]))
         outs[-1].start()
 
-    put(rows_ref, rows_out)
-    put(cot_ref, cot_out)
-    put(rec_ref, rec_out)
-    put(lru_ref, lru_out)
-    put(stats, gain_out)
     strip = 32
 
     def activate(i, c):
@@ -405,47 +479,98 @@
         du[at, :] = (d_hidden * silu).astype(BF16)
         return c
 
+    def back_to(k, lo, hi, store):
+        def columns(at, size):
+            here = pl.ds(pl.multiple_of(k * feat + at, LANE), size)
+            store(
+                pl.ds(at, size),
+                mm(dg[lo:hi, :], wg[here, :], 1, 1) + mm(du[lo:hi, :], wu[here, :], 1, 1),
+            )
+
+        in_blocks(columns, feat)
+
     slots = rows_ref.shape[0]
-    lax.fori_loop(0, slots // strip, activate, 0)
+    crossing = []
+
+    def finish_far(h):
+        lo, hi = (wide, slots) if h else (0, wide)
+        for i in range(h * quad, (h + 1) * quad):
+            pass_far(far, i, right).wait_recv()
+            for k in range(per):
+                source = group_of(i) * per + k
+                if i == 0:
+
+                    @pl.when(source != me)
+                    def _():
+                        handed(source).wait_recv()
+                else:
+                    handed(source).wait_recv()
+        place(far, lambda rows: recv_far[rows, :], (h,), h == 1)
+        if h == 1:
+            put(rows_ref, rows_out)
+            put(cot_ref, cot_out)
+            put(rec_ref, rec_out)
+            put(lru_ref, lru_out)
+            put(stats, gain_out)
+        contract(far, lo, hi, False)
+        lax.fori_loop(lo // strip, hi // strip, activate, 0)
+
+        def to_far(here, value):
+            far_out[lo:hi, here] = value.astype(BF16)
+
+        back_to(far, lo, hi, to_far)
+        cut = (hi - lo) // 2
+        for n, (at, to) in enumerate(((lo, right), (lo + cut, left))):
+            rows = pl.ds(at, cut)
+            c = copy_to(
+                far_out.at[rows], far_in.at[rows], f_send.at[2 * h + n], f_recv.at[2 * h + n], me, to
+            )
+            c.start()
+            crossing.append((c, n, at, at + cut))
+
+    def finish_near(h):
+        lo, hi = (wide, slots) if h else (0, wide)
+
+        def to_own(here, value):
+            own_sum[lo:hi, here] = value.astype(BF16)
+
+        def to_right(here, value):
+            right_dx[lo:hi, here] = value
+
+        def to_left(here, value):
+            left_dx[lo:hi, here] = value
+
+        back_to(tp, lo, hi, to_own)
+        back_to(right, lo, hi, to_right)
+        back_to(left, lo, hi, to_left)
+
+    finish_far(0)
+    relay(quad)
+    relay(quad + 1)
+    finish_near(0)
+    relay(quad + 2)
+    relay(quad + 3)
+    near_half(left, 1, 1, l_send, fl_recv, right)
+    near_half(right, 1, 0, r_send, fr_recv, left)
+    finish_far(1)
     put(hid, hid_out)
     put(dg, dg_out)
     put(du, du_out)
-
-    def back_to(k, store):
-        def columns(at, size):
-            here = pl.ds(pl.multiple_of(k * feat + at, LANE), size)
-            store(at, size, mm(dg[...], wg[here, :], 1, 1) + mm(du[...], wu[here, :], 1, 1))
-
-        in_blocks(columns, feat)
-
-    def into(ref, kind):
-        def store(at, size, value):
-            ref[:, pl.ds(at, size)] = value.astype(kind)
-
-        return store
-
-    half = slots // 2
-    back_to(far, into(far_out, BF16))
-    top, low = pl.ds(0, half), pl.ds(half, half)
-    for n, (rows, to) in enumerate(((top, right), (low, left))):
-        c = copy_to(far_out.at[rows], far_in.at[rows], f_send.at[n], f_recv.at[n], me, to)
-        c.start()
-        started.append(c)
-    back_to(tp, into(own_sum, BF16))
+    finish_near(1)
     put(own_sum, own_out)
-    back_to(right, into(acc_g, F32))
-    back_to(left, into(acc_u, F32))
-    fwd_sum[half:, :] = acc_g[half:, 0:feat].astype(BF16)
-    bwd_sum[0:half, :] = acc_u[0:half, 0:feat].astype(BF16)
-    for c in started[-2:]:
+    for c, n, lo, hi in crossing:
+        mine = bwd_sum if n == 0 else fwd_sum
+        total = fwd_sum if n == 0 else bwd_sum
+        mine[lo:hi, :] = (left_dx if n == 0 else right_dx)[lo:hi, :].astype(BF16)
         c.wait_recv()
-    fwd_sum[0:half, :] = (acc_g[0:half, 0:feat] + far_in[0:half, :].astype(F32)).astype(BF16)
-    bwd_sum[half:, :] = (acc_u[half:, 0:feat] + far_in[half:, :].astype(F32)).astype(BF16)
+        total[lo:hi, :] = (
+            (right_dx if n == 0 else left_dx)[lo:hi, :] + far_in[lo:hi, :].astype(F32)
+        ).astype(BF16)
     put(fwd_sum, fwd_out)
     put(bwd_sum, bwd_out)
     for c in outs:
         c.wait()
-    for c in sends + told + started:
+    for c in first_hop + next_hop + sends + told + started + [c[0] for c in crossing]:
         c.wait_send()
 
 
@@ -479,6 +604,15 @@
         scratch_shapes=[
             pltpu.VMEM((n_sp * MAIN, width), BF16),
             pltpu.VMEM((4, n_sp * MAIN, width), BF16),
+            pltpu.VMEM((n_sp * MAIN, tokens), BF16),
+            pltpu.VMEM((2, tokens // 2, feat), BF16),
+            pltpu.VMEM((tokens, feat), BF16),
+            pltpu.VMEM((n_sp * MAIN, feat), BF16),
+            pltpu.VMEM((n_sp * MAIN, feat), BF16),
+            dma((4,)),
+            dma((4,)),
+            dma((n_sp,)),
+            dma((n_sp,)),
             pltpu.VMEM((n_sp * MAIN, LANE), F32),
             pltpu.VMEM((1, 2, chans), F32),
             pltpu.VMEM((n_sp, 2, chans), F32),
@@ -495,6 +629,8 @@
             pltpu.VMEM((slots, hidden), BF16),
             pltpu.VMEM((slots, feat), BF16),
             pltpu.VMEM((slots, feat), BF16),
+            pltpu.VMEM((slots, feat), F32),
+            pltpu.VMEM((slots, feat), F32),
             pltpu.VMEM((slots, feat), BF16),
             pltpu.VMEM((slots, feat), BF16),
             pltpu.VMEM((slots, feat), BF16),
@@ -502,8 +638,8 @@
             pltpu.VMEM((tokens, chans), BF16),
             dma((3,)),
             dma((11,)),
-            dma((2,)),
-            dma((2,)),
+            dma((4,)),
+            dma((4,)),
             dma((n_sp,)),
             dma((n_sp,)),
             dma,
@@ -542,7 +678,6 @@
     sg_ref,
     rext,
     arr,
-    arrx,
     full,
     prod,
     pair,
@@ -552,14 +687,13 @@
     terms,
     m_send,
     m_recv,
-    x_send,
-    x_recv,
     own_sems,
     a_send,
     fl_recv,
     fr_recv,
     ff_recv,
-    p_sems,
+    p_send,
+    p_recv,
     o_send,
     o_recv,
     t_send,
@@ -574,16 +708,20 @@
     tokens, feat = og_ref.shape
     extra = 2
     cuts = feat // LANE
-    xrows = extra * cuts
     greet([(lax.rem(me + d, n_sp), tp) for d in range(1, n_sp)] + [(me, right), (me, left)])
 
     main = n_sp * MAIN
-    sg_ref[...] = (
-        own_ref[...].astype(F32) + (fwd_ref[...].astype(F32) + bwd_ref[...].astype(F32))
-    ).astype(BF16)
-    sx = sg_ref[main:, :].astype(F32)
+    total = own_ref[...].astype(F32) + (fwd_ref[...].astype(F32) + bwd_ref[...].astype(F32))
+    sg_ref[:, 0:feat] = total[0:main, :].astype(BF16)
+    rext[...] = jnp.zeros_like(rext)
     for b in range(cuts):
-        rext[pl.ds(b, n_sp * extra, stride=cuts), :] = sx[:, b * LANE : (b + 1) * LANE]
+        rext[pl.ds(b, n_sp * extra, stride=2 * cuts), :] = total[main:, b * LANE : (b + 1) * LANE]
+    wide = main // 2
+    for h in (0, 1):
+        source_half = lax.rem(me // (n_sp // 2) + h, 2)
+        sg_ref[h * wide : (h + 1) * wide, feat : feat + LANE] = rext[
+            pl.ds(pl.multiple_of(source_half * wide, wide), wide), :
+        ].astype(BF16)
     r0 = routes_ref[:, 0:1].astype(F32)
     r1 = routes_ref[:, 1:2].astype(F32)
     expert = iota((tokens, n_sp), 1)
@@ -608,105 +746,114 @@
     def rows_of(index, size):
         return pl.ds(pl.multiple_of(index * size, size), size)
 
-    own = [
-        pltpu.make_async_copy(
-            sg_ref.at[rows_of(me, MAIN)], arr.at[rows_of(me, MAIN)], own_sems.at[0]
-        ),
-        pltpu.make_async_copy(
-            rext.at[rows_of(me, xrows)], arrx.at[rows_of(me, xrows)], own_sems.at[1]
-        ),
-    ]
-    sends = []
-    for d in range(1, n_sp):
-        peer = lax.rem(me + d, n_sp)
-        sends.append(
-            copy_to(
-                sg_ref.at[rows_of(peer, MAIN)],
-                arr.at[rows_of(me, MAIN)],
-                m_send.at[d],
-                m_recv.at[me],
-                peer,
-                tp,
-            )
-        )
-        sends.append(
-            copy_to(
-                rext.at[rows_of(peer, xrows)],
-                arrx.at[rows_of(me, xrows)],
-                x_send.at[d],
-                x_recv.at[me],
-                peer,
-                tp,
-            )
-        )
-    for c in own + sends:
-        c.start()
-    for c in own:
-        c.wait()
-    for d in range(1, n_sp):
-        source = lax.rem(me + n_sp - d, n_sp)
-        copy_to(
-            sg_ref.at[rows_of(source, MAIN)],
+    def held_for(peer):
+        half = n_sp // 2
+        at = lax.rem(peer // half + me // half, 2) * half + lax.rem(peer, half)
+        return rows_of(at, MAIN)
+
+    own = pltpu.make_async_copy(
+        sg_ref.at[held_for(me)], arr.at[rows_of(me, MAIN)], own_sems.at[0]
+    )
+
+    def give(d, peer, source):
+        return copy_to(
+            sg_ref.at[held_for(peer)],
             arr.at[rows_of(source, MAIN)],
             m_send.at[d],
             m_recv.at[source],
-            source,
+            peer,
             tp,
-        ).wait_recv()
-        copy_to(
-            rext.at[rows_of(source, xrows)],
-            arrx.at[rows_of(source, xrows)],
-            x_send.at[d],
-            x_recv.at[source],
-            source,
-            tp,
-        ).wait_recv()
-    back = mm(pick, arr[...])
-    backx = jnp.concatenate(
-        [mm(pickx, arrx[pl.ds(b, n_sp * extra, stride=cuts), :].astype(BF16)) for b in range(cuts)],
-        axis=1,
-    )
-    full[tp] = (og_ref[...].astype(F32) + (back + backx)).astype(BF16)
+        )
+
+    sends = [give(d, lax.rem(me + d, n_sp), me) for d in range(1, n_sp)]
+    own.start()
+    for c in sends:
+        c.start()
+    own.wait()
 
     half = tokens // 2
 
     def piece(quarter, h, send_sem, recv_sem, to):
         ref = full.at[quarter, pl.ds(h * half, half)]
-        return copy_to(ref, ref, send_sem, recv_sem, me, to)
-
+        return copy_to(ref, ref, a_send.at[send_sem], recv_sem, me, to)
+
+    def from_left(h):
+        return piece(left, h, 0, fl_recv.at[h], right)
+
+    def from_right(h):
+        return piece(right, h, 0, fr_recv.at[h], left)
+
+    for d in range(1, n_sp):
+        source = lax.rem(me + n_sp - d, n_sp)
+        give(d, source, source).wait_recv()
+    rext[...] = arr[:, feat : feat + LANE].astype(F32)
     for h in (0, 1):
-        sends.append(piece(tp, h, a_send.at[h], fl_recv.at[h], right))
-        sends.append(piece(tp, 1 - h, a_send.at[3 - h], fr_recv.at[1 - h], left))
-        sends[-2].start()
+        rows = slice(h * half, (h + 1) * half)
+        back = mm(pick[rows, :], arr[:, 0:feat])
+        backx = jnp.concatenate(
+            [
+                mm(pickx[rows, :], rext[pl.ds(b, n_sp * extra, stride=2 * cuts), :].astype(BF16))
+                for b in range(cuts)
+            ],
+            axis=1,
+        )
+        full[tp, rows, :] = (og_ref[rows, :].astype(F32) + (back + backx)).astype(BF16)
+    for h in (0, 1):
+        sends.append(piece(tp, h, h, fl_recv.at[h], right))
         sends[-1].start()
+        sends.append(piece(tp, 1 - h, 2 + h, fr_recv.at[1 - h], left))
+        sends[-1].start()
 
     lru = lru_ref[...]
-
-    def use(quarter):
+    share = chips // 4
+
+    def use(quarter, n):
         part = full[quarter]
-        wide = mm(part, lru, 0, 0).astype(BF16)
-        prod[pl.ds(quarter * (chips // 4), chips // 4)] = wide.reshape(
-            chips // 4, 2, wide.shape[0] // (chips // 2), wide.shape[1]
+        spread = mm(part, lru, 0, 0).astype(BF16)
+        mine = pl.ds(quarter * share, share)
+        prod[mine] = spread.reshape(share, 2, feat // (2 * share), spread.shape[1])
+        trade(quarter, n).start()
+        return mm(part, wout_ref[pl.ds(pl.multiple_of(quarter * feat, feat), feat), :])
+
+    def trade(quarter, n):
+        mine = pl.ds(quarter * share, share)
+        return copy_to(
+            prod.at[mine, 1 - core], pair.at[mine], p_send.at[n], p_recv.at[n], partner, tp
         )
-        return mm(part, wout_ref[pl.ds(pl.multiple_of(quarter * feat, feat), feat), :])
-
-    mixer = use(tp)
-    piece(left, 0, a_send.at[0], fl_recv.at[0], right).wait_recv()
-    sends.append(piece(left, 0, a_send.at[4], ff_recv.at[0], right))
+
+    def to_owner(at, source):
+        return copy_to(
+            summed.at[at], owned.at[source], o_send.at[at], o_recv.at[source], at * 2 + core, tp
+        )
+
+    def settle(quarter, n):
+        trade(quarter, n).wait_recv()
+        mine = pl.ds(quarter * share, share)
+        summed[mine] = (prod[mine, core].astype(F32) + pair[mine].astype(F32)).astype(BF16)
+        for k in range(share):
+            at = quarter * share + k
+
+            @pl.when(at != chip)
+            def _():
+                to_owner(at, chip).start()
+
+    mixer = use(tp, 0)
+    from_left(0).wait_recv()
+    sends.append(piece(left, 0, 4, ff_recv.at[0], right))
     sends[-1].start()
-    piece(right, 1, a_send.at[0], fr_recv.at[1], left).wait_recv()
-    sends.append(piece(right, 1, a_send.at[5], ff_recv.at[1], left))
+    from_right(1).wait_recv()
+    sends.append(piece(right, 1, 5, ff_recv.at[1], left))
     sends[-1].start()
-    piece(left, 1, a_send.at[0], fl_recv.at[1], right).wait_recv()
-    mixer = mixer + use(left)
-    piece(right, 0, a_send.at[0], fr_recv.at[0], left).wait_recv()
-    mixer = mixer + use(right)
-    piece(far, 0, a_send.at[0], ff_recv.at[0], right).wait_recv()
-    piece(far, 1, a_send.at[0], ff_recv.at[1], left).wait_recv()
-    mixer = mixer + use(far)
-
-    trade = copy_to(prod.at[:, 1 - core], pair, p_sems.at[0], p_sems.at[1], partner, tp)
-    trade.start()
+    settle(tp, 0)
+    from_left(1).wait_recv()
+    mixer = mixer + use(left, 1)
+    from_right(0).wait_recv()
+    mixer = mixer + use(right, 2)
+    settle(left, 1)
+    settle(right, 2)
+    for h in (0, 1):
+        piece(far, h, 0, ff_recv.at[h], right).wait_recv()
+    mixer = mixer + use(far, 3)
 
     decay = rec_ref[0]
     row = lax.broadcasted_iota(jnp.int32, decay.shape, 0)
@@ -723,16 +870,7 @@
         )
         sends[-1].start()
 
-    trade.wait()
-    summed[...] = (prod[:, core].astype(F32) + pair[...].astype(F32)).astype(BF16)
-    for d in range(1, chips):
-        to = lax.rem(chip + d, chips)
-        sends.append(
-            copy_to(
-                summed.at[to], owned.at[chip], o_send.at[d], o_recv.at[chip], to * 2 + core, tp
-            )
-        )
-        sends[-1].start()
+    settle(far, 3)
     owned[chip] = summed[chip]
 
     for d in range(1, n_sp):
@@ -756,18 +894,15 @@
 
     for d in range(1, chips):
         source = lax.rem(chip + chips - d, chips)
-        copy_to(
-            summed.at[source],
-            owned.at[source],
-            o_send.at[d],
-            o_recv.at[source],
-            source * 2 + core,
-            tp,
-        ).wait_recv()
+        to_owner(source, source).wait_recv()
     total = owned[0].astype(F32)
     for j in range(1, chips):
         total = total + owned[j].astype(F32)
     gop_ref[...] = total
+    for n, quarter in enumerate((tp, left, right, far)):
+        trade(quarter, n).wait_send()
+    for d in range(1, chips):
+        to_owner(lax.rem(chip + d, chips), chip).wait_send()
     for c in sends:
         c.wait_send()
 
@@ -779,7 +914,6 @@
     share = wout.shape[0] // n_sp
     vmem = pl.BlockSpec(memory_space=pltpu.VMEM)
     dma = pltpu.SemaphoreType.DMA
-    xrows = 2 * feat // LANE
     return pl.pallas_call(
         functools.partial(tail_kernel, n_sp),
         out_shape=(
@@ -790,10 +924,9 @@
         in_specs=[vmem] * 11,
         out_specs=(vmem,) * 3,
         scratch_shapes=[
-            pltpu.VMEM(own.shape, BF16),
-            pltpu.VMEM((n_sp * xrows, LANE), F32),
-            pltpu.VMEM((n_sp * MAIN, feat), BF16),
-            pltpu.VMEM((n_sp * xrows, LANE), F32),
+            pltpu.VMEM((n_sp * MAIN, feat + LANE), BF16),
+            pltpu.VMEM((n_sp * MAIN, LANE), F32),
+            pltpu.VMEM((n_sp * MAIN, feat + LANE), BF16),
             pltpu.VMEM((4, tokens, feat), BF16),
             pltpu.VMEM((chips, 2, share, chans), BF16),
             pltpu.VMEM((chips, share, chans), BF16),
@@ -803,14 +936,13 @@
             pltpu.VMEM((n_sp, 1, chans), F32),
             dma((n_sp,)),
             dma((n_sp,)),
-            dma((n_sp,)),
-            dma((n_sp,)),
-            dma((2,)),
+            dma((1,)),
             dma((6,)),
             dma((2,)),
             dma((2,)),
             dma((2,)),
-            dma((2,)),
+            dma((4,)),
+            dma((4,)),
             dma((chips,)),
             dma((chips,)),
             dma((n_sp,)),
@@ -821,6 +953,55 @@
         ),
         name="tail",
     )(own, fwd, bwd, og, routes, wout, wr, wi, rec, lru, gains)
+
+
+def into_weights_kernel(x_ref, dg_ref, du_ref, gate_ref, up_ref):
+    flipped = jnp.transpose(x_ref[...])
+    gate_ref[...] = mm(flipped, dg_ref[...]).astype(BF16)
+    up_ref[...] = mm(flipped, du_ref[...]).astype(BF16)
+
+
+def from_weights_kernel(h_ref, c_ref, down_ref, flipped):
+    @pl.when(pl.program_id(0) == 0)
+    def _():
+        flipped[...] = jnp.transpose(h_ref[...])
+
+    down_ref[...] = mm(flipped[...], c_ref[...]).astype(BF16)
+
+
+def weight_gradients(x, cot, hid, dg, du, block=512):
+    slots, width = x.shape
+    hidden = hid.shape[1]
+    whole = pl.BlockSpec((slots, hidden), lambda i: (0, 0))
+    strip = pl.BlockSpec((slots, block), lambda i: (0, i))
+    flops = 2 * slots * width * hidden
+
+    def cost(n):
+        moved = 2 * (slots * width + n * slots * hidden + n * width * hidden)
+        return pl.CostEstimate(flops=n * flops, bytes_accessed=moved, transcendentals=0)
+
+    gate, up = pl.pallas_call(
+        into_weights_kernel,
+        grid=(width // block,),
+        out_shape=(jax.ShapeDtypeStruct((width, hidden), BF16),) * 2,
+        in_specs=[strip, whole, whole],
+        out_specs=(pl.BlockSpec((block, hidden), lambda i: (i, 0)),) * 2,
+        compiler_params=pltpu.CompilerParams(vmem_limit_bytes=40 * 1024 * 1024),
+        cost_estimate=cost(2),
+        name="grads_into",
+    )(x, dg, du)
+    down = pl.pallas_call(
+        from_weights_kernel,
+        grid=(width // block,),
+        out_shape=jax.ShapeDtypeStruct((hidden, width), BF16),
+        in_specs=[whole, strip],
+        out_specs=pl.BlockSpec((hidden, block), lambda i: (0, i)),
+        scratch_shapes=[pltpu.VMEM((hidden, slots), BF16)],
+        compiler_params=pltpu.CompilerParams(vmem_limit_bytes=67043328),
+        cost_estimate=cost(1),
+        name="grads_from",
+    )(hid, cot)
+    return gate, up, down
 
 
 def per_device(
@@ -858,9 +1039,7 @@
     )
     fwd = lax.ppermute(fwd, "tp", [(k, (k + 1) % 4) for k in range(4)])
     bwd = lax.ppermute(bwd, "tp", [(k, (k + 3) % 4) for k in range(4)])
-    grad_down = mm(hidden, cotangent, 0, 0).astype(BF16)
-    grad_gate = mm(inputs, d_gate, 0, 0).astype(BF16)
-    grad_up = mm(inputs, d_up, 0, 0).astype(BF16)
+    grad_gate, grad_up, grad_down = weight_gradients(inputs, cotangent, hidden, d_gate, d_up)
     grad_out_proj, grad_input, grad_gate_pre = tail(
         n_sp,
         own,

time: 134 us -> 127 us (0.948); the launches traced: 131 us -> 127 us
  matrix products: 18.8 us -> 0 us
  Pallas kernels: 108 us -> 118 us
  local copies, waits for them, and re-layouts: 2.16 us -> 6.9 us
    dot_general x3 -> x0, matrix products: 18.8 us -> none  [mm(): lax.dot_general(a, b, (((ca,), (cb,)), ((), ())), preferred_element_type=...]
    pallas_call x0 -> x2, Pallas kernels: none -> 15 us  [the longest x1 8.22 us: weight_gradients(): pl.pallas_call(into_weights_kernel, grid=(width // block,), out_shape=(ja...]
    unnamed x28 -> x30, local copies, waits for them, and re-layouts: 2.16 us -> 6.9 us
    pallas_call x1, Pallas kernels: 67.7 us -> 63.9 us  [dispatch(): pl.pallas_call(functools.partial(dispatch_kernel, n_sp), out_shape=(shape...]
    pallas_call x1, Pallas kernels: 40.5 us -> 38.6 us  [tail(): pl.pallas_call(functools.partial(tail_kernel, n_sp), out_shape=(jax.Shape...]
  transfers between devices with their start and end apart: 2 -> 2, of which waited for: 0 -> 0; matrix products, arithmetic and copies ran while one was open for 14% -> 1% of each run, Pallas kernels for 0% -> 12%
where the time goes in v2:
time: 127 us
  Pallas kernels  118 us (93%)
  local copies, waits for them, and re-layouts  6.9 us (5%)
  starting transfers between devices  1.71 us (1%)
    pallas_call x1, Pallas kernels, dispatch(): pl.pallas_call(functools.partial(dispatch_kernel, n_sp), out_shape=(shape...  63.9 us
    pallas_call x1, Pallas kernels, tail(): pl.pallas_call(functools.partial(tail_kernel, n_sp), out_shape=(jax.Shape...  38.6 us
    pallas_call x1, Pallas kernels, weight_gradients(): pl.pallas_call(into_weights_kernel, grid=(width // block,), out_shape=(ja...  8.22 us
    unnamed x30, local copies, waits for them, and re-layouts  6.9 us
    pallas_call x1, Pallas kernels, weight_gradients(): pl.pallas_call(from_weights_kernel, grid=(width // block,), out_shape=jax...  6.81 us
  transfers between devices with their start and end apart: 2, of which 0 were waited for; matrix products, arithmetic and copies ran while one was open for 1% of the time, Pallas kernels for 12%

profile of v2, /device:TPU:27, one launch (start us, length us, event | category | flops | bytes accessed | tf_op | source)
XLA Modules:
  0.0 126.9 jit_solution(12141015086632279032)
XLA Ops:
  0.6 0.0 copy-start.12
  0.6 63.9 %dispatch.1 = (bf16[576,2048]{1,0:T(8,128)(2,1)}, bf16[576,2048]{1,0:T(8,128)(2,1)}, bf16[576,896]{1,0:T(8,128)(2,1)}, bf16[576,896]{1,0:T(8,128)(2,1)}, bf16[57...) custom-call(bf16[192,512]{1,0:T(8,128)(2,1)} %x_ref.1, ...), custom_call_target="tpu_custom_call" | custom-call | tf_op jit(solution)/shard_map/dispatch/pallas_call | solution.py:587
  64.5 0.3 collective-permute-start
  64.8 1.5 %collective-permute-start.1 = (bf16[576,512]{1,0:T(8,128)(2,1)}, bf16[576,512]{1,0:T(8,128)(2,1)}, u32[]{:S(2)}, u32[]{:S(2)}) collective-permute-start(bf16[576,512]{1,0:T(8,128)(2,1)} %get-tuple-element.31), channel_id=1, source_target_pairs={{0,3},{1,0},{2,1},{3,2},{4,7},{5,4},{6,5},{7,6},{8,11},{9,8},{10,9... | collective-permute-start | bytes 1769480 | tf_op jit(solution)/shard_map/ppermute | solution.py:1041
  66.3 0.0 copy-done.12
  66.3 0.8 copy.20.routes_ref
  67.0 6.8 %grads_from.1 = bf16[896,2048]{1,0:T(8,128)(2,1)} custom-call(bf16[576,896]{1,0:T(8,128)(2,1)} %get-tuple-element.27.h_ref, bf16[576,2048]{1,0:T(8,128)(2,1)} %get-tuple-element.28.c_ref), custom_call_target="tpu_custom_call" | custom-call | flops 2113929216 | bytes 7061504 | tf_op jit(solution)/shard_map/grads_from/pallas_call | solution.py:993
  73.8 0.0 copy-start.9
  73.8 1.7 %copy-done.9 = bf16[576,2048]{1,0:T(8,128)(2,1)S(1)} copy-done((bf16[576,2048]{1,0:T(8,128)(2,1)S(1)}, bf16[576,2048]{1,0:T(8,128)(2,1)}, u32[]{:S(2)}) %copy-start.9) | copy-done | bytes 2359320
  75.5 1.2 copy-done.10
  76.7 1.2 copy-done.11
  77.9 0.0 copy-start.4
  78.0 0.0 copy-start.5
  78.0 0.0 copy-start.6
  78.0 0.0 copy-start.7
  78.0 0.0 copy-start.8
  78.0 8.2 %grads_into.1 = (bf16[2048,896]{1,0:T(8,128)(2,1)}, bf16[2048,896]{1,0:T(8,128)(2,1)}) custom-call(bf16[576,2048]{1,0:T(8,128)(2,1)S(1)} %copy-done.9, bf16[576,896]{1,0:T(8,128)(2,1)S(1)} %copy-done.10, bf16[576,896]{1,0:T(8,128)(2,1)S(1)} %copy-done.11), custom_call_target="tpu_custom_call" | custom-call | flops 4227858432 | bytes 11763712 | tf_op jit(solution)/shard_map/grads_into/pallas_call | solution.py:983
  86.2 0.0 collective-permute-done.fwd_ref
  86.2 0.0 collective-permute-done.1.bwd_ref
  86.2 0.0 copy-done
  86.2 0.0 copy-done.1
  86.2 0.0 copy-done.2
  86.3 0.0 copy-done.3
  86.3 0.0 copy-done.4
  86.3 0.0 copy-done.5
  86.3 0.0 copy-done.6
  86.3 0.0 copy-done.7
  86.3 0.0 copy-done.8
  86.3 38.6 %tail.1 = (f32[64,256]{1,0:T(8,128)S(1)}, f32[192,256]{1,0:T(8,128)S(1)}, f32[192,256]{1,0:T(8,128)S(1)}) custom-call(bf16[576,512]{1,0:T(8,128)(2,1)S(1)} %copy-done.5, bf16[576,512]{1,0:T(8,128)(2,1)} %collective-permute-done.fwd_ref, bf16[576,512]{1,0:T(8,128)(2,1)} %collective-permute-done.1.bwd_ref, bf16[192,512]{1,0:T(8,128)(2,1)S(1)} %copy-done.4, ...), custom_call_target="tpu_custom_call" | custom-call | tf_op jit(solution)/shard_map/tail/pallas_call | solution.py:917
  124.9 0.6 copy.24
  125.6 0.7 copy.25
  126.2 0.7 copy.26
  (6 shorter events, 0.0 us)
Async XLA Ops:
  0.6 65.6 %copy-start.12 = (s32[192,2]{0,1:T(2,128)S(1)}, s32[192,2]{0,1:T(2,128)}, u32[]{:S(2)}) copy-start(s32[192,2]{0,1:T(2,128)} %param.16) | copy-start | bytes 4612
  64.5 21.7 %collective-permute-start = (bf16[576,512]{1,0:T(8,128)(2,1)}, bf16[576,512]{1,0:T(8,128)(2,1)}, u32[]{:S(2)}, u32[]{:S(2)}) collective-permute-start(bf16[576,512]{1,0:T(8,128)(2,1)} %get-tuple-element.30), channel_id=1, source_target_pairs={{0,1},{1,2},{2,3},{3,0},{4,5},{5,6},{6,7},{7,4},{8,9},{9,10},{10,1... | collective-permute-start | bytes 1769480 | tf_op jit(solution)/shard_map/ppermute | solution.py:1040
  64.8 21.4 %collective-permute-start.1 = (bf16[576,512]{1,0:T(8,128)(2,1)}, bf16[576,512]{1,0:T(8,128)(2,1)}, u32[]{:S(2)}, u32[]{:S(2)}) collective-permute-start(bf16[576,512]{1,0:T(8,128)(2,1)} %get-tuple-element.31), channel_id=1, source_target_pairs={{0,3},{1,0},{2,1},{3,2},{4,7},{5,4},{6,5},{7,6},{8,11},{9,8},{10,9... | collective-permute-start | bytes 1769480 | tf_op jit(solution)/shard_map/ppermute | solution.py:1041
  73.8 1.7 %copy-start.9 = (bf16[576,2048]{1,0:T(8,128)(2,1)S(1)}, bf16[576,2048]{1,0:T(8,128)(2,1)}, u32[]{:S(2)}) copy-start(bf16[576,2048]{1,0:T(8,128)(2,1)} %get-tuple-element.22.x_ref) | copy-start | bytes 7077892
  75.5 1.2 copy-start.10
  76.7 1.2 copy-start.11
  77.9 8.3 %copy-start = (f32[6,192,256]{2,1,0:T(8,128)S(1)}, f32[6,192,256]{2,1,0:T(8,128)}, u32[]{:S(2)}) copy-start(f32[6,192,256]{2,1,0:T(8,128)} %get-tuple-element.32.rec_ref) | copy-start | bytes 3538948
  77.9 8.3 %copy-start.1 = (bf16[2048,256]{1,0:T(8,128)(2,1)S(1)}, bf16[2048,256]{1,0:T(8,128)(2,1)}, u32[]{:S(2)}) copy-start(bf16[2048,256]{1,0:T(8,128)(2,1)} %wout_ref.1) | copy-start | bytes 3145732
  77.9 8.3 %copy-start.2 = (bf16[8,128,128]{2,1,0:T(8,128)(2,1)S(1)}, bf16[8,128,128]{2,1,0:T(8,128)(2,1)}, u32[]{:S(2)}) copy-start(bf16[8,128,128]{2,1,0:T(8,128)(2,1)} %wr_ref.3) | copy-start | bytes 786436
  77.9 8.3 %copy-start.3 = (bf16[8,128,128]{2,1,0:T(8,128)(2,1)S(1)}, bf16[8,128,128]{2,1,0:T(8,128)(2,1)}, u32[]{:S(2)}) copy-start(bf16[8,128,128]{2,1,0:T(8,128)(2,1)} %wi_ref.3) | copy-start | bytes 786436
  77.9 8.3 %copy-start.4 = (bf16[192,512]{1,0:T(8,128)(2,1)S(1)}, bf16[192,512]{1,0:T(8,128)(2,1)}, u32[]{:S(2)}) copy-start(bf16[192,512]{1,0:T(8,128)(2,1)} %og_ref.1) | copy-start | bytes 589828
  78.0 8.3 %copy-start.5 = (bf16[576,512]{1,0:T(8,128)(2,1)S(1)}, bf16[576,512]{1,0:T(8,128)(2,1)}, u32[]{:S(2)}) copy-start(bf16[576,512]{1,0:T(8,128)(2,1)} %get-tuple-element.29.own_ref) | copy-start | bytes 1769476
  78.0 8.3 %copy-start.6 = (s32[192,2]{1,0:T(8,128)S(1)}, s32[192,2]{1,0:T(8,128)}, u32[]{:S(2)}) copy-start(s32[192,2]{1,0:T(8,128)} %copy.20.routes_ref) | copy-start | bytes 4612
  78.0 8.3 %copy-start.7 = (bf16[192,256]{1,0:T(8,128)(2,1)S(1)}, bf16[192,256]{1,0:T(8,128)(2,1)}, u32[]{:S(2)}) copy-start(bf16[192,256]{1,0:T(8,128)(2,1)} %get-tuple-element.33.lru_ref) | copy-start | bytes 294916
  78.0 8.3 %copy-start.8 = (f32[32,2,256]{2,1,0:T(2,128)S(1)}, f32[32,2,256]{2,1,0:T(2,128)}, u32[]{:S(2)}) copy-start(f32[32,2,256]{2,1,0:T(2,128)} %get-tuple-element.34.gain_ref) | copy-start | bytes 196612

commit v3 on v2

--- a/solution.py
+++ b/solution.py
@@ -525,7 +525,6 @@
             c = copy_to(
                 far_out.at[rows], far_in.at[rows], f_send.at[2 * h + n], f_recv.at[2 * h + n], me, to
             )
-            c.start()
             crossing.append((c, n, at, at + cut))
 
     def finish_near(h):
@@ -550,9 +549,13 @@
     finish_near(0)
     relay(quad + 2)
     relay(quad + 3)
+    for c in crossing:
+        c[0].start()
     near_half(left, 1, 1, l_send, fl_recv, right)
     near_half(right, 1, 0, r_send, fr_recv, left)
     finish_far(1)
+    for c in crossing[2:]:
+        c[0].start()
     put(hid, hid_out)
     put(dg, dg_out)
     put(du, du_out)
@@ -838,13 +841,13 @@
                 to_owner(at, chip).start()
 
     mixer = use(tp, 0)
+    settle(tp, 0)
     from_left(0).wait_recv()
     sends.append(piece(left, 0, 4, ff_recv.at[0], right))
     sends[-1].start()
     from_right(1).wait_recv()
     sends.append(piece(right, 1, 5, ff_recv.at[1], left))
     sends[-1].start()
-    settle(tp, 0)
     from_left(1).wait_recv()
     mixer = mixer + use(left, 1)
     from_right(0).wait_recv()
@@ -997,7 +1000,7 @@
         in_specs=[whole, strip],
         out_specs=pl.BlockSpec((hidden, block), lambda i: (0, i)),
         scratch_shapes=[pltpu.VMEM((hidden, slots), BF16)],
-        compiler_params=pltpu.CompilerParams(vmem_limit_bytes=67043328),
+        compiler_params=pltpu.CompilerParams(vmem_limit_bytes=40 * 1024 * 1024),
         cost_estimate=cost(1),
         name="grads_from",
     )(hid, cot)

time: 127 us -> 120 us (0.945)
  Pallas kernels: 118 us -> 113 us
  local copies, waits for them, and re-layouts: 6.9 us -> 5.04 us
    pallas_call x1, Pallas kernels: 63.9 us -> 61.8 us  [dispatch(): pl.pallas_call(functools.partial(dispatch_kernel, n_sp), out_shape=(shape...]
    unnamed x30 -> x32, local copies, waits for them, and re-layouts: 6.9 us -> 5.04 us
    pallas_call x1, Pallas kernels: 6.81 us -> 5.03 us  [weight_gradients(): pl.pallas_call(from_weights_kernel, grid=(width // block,), out_shape=jax...]
  transfers between devices with their start and end apart: 2 -> 2, of which waited for: 0 -> 0; matrix products, arithmetic and copies ran while one was open for 1% -> 0% of each run, Pallas kernels for 12% -> 11%
where the time goes in v3:
time: 120 us
  Pallas kernels  113 us (94%)
  local copies, waits for them, and re-layouts  5.04 us (4%)
  starting transfers between devices  1.53 us (1%)
    pallas_call x1, Pallas kernels, dispatch(): pl.pallas_call(functools.partial(dispatch_kernel, n_sp), out_shape=(shape...  61.8 us
    pallas_call x1, Pallas kernels, tail(): pl.pallas_call(functools.partial(tail_kernel, n_sp), out_shape=(jax.Shape...  37.8 us
    pallas_call x1, Pallas kernels, weight_gradients(): pl.pallas_call(into_weights_kernel, grid=(width // block,), out_shape=(ja...  8.23 us
    unnamed x32, local copies, waits for them, and re-layouts  5.04 us
    pallas_call x1, Pallas kernels, weight_gradients(): pl.pallas_call(from_weights_kernel, grid=(width // block,), out_shape=jax...  5.03 us
  transfers between devices with their start and end apart: 2, of which 0 were waited for; matrix products, arithmetic and copies ran while one was open for 0% of the time, Pallas kernels for 11%

profile of v3, /device:TPU:27, one launch (start us, length us, event | category | flops | bytes accessed | tf_op | source)
XLA Modules:
  0.0 120.2 jit_solution(11294862841579637162)
XLA Ops:
  0.6 0.0 copy-start.13
  0.6 61.8 %dispatch.1 = (bf16[576,2048]{1,0:T(8,128)(2,1)}, bf16[576,2048]{1,0:T(8,128)(2,1)}, bf16[576,896]{1,0:T(8,128)(2,1)}, bf16[576,896]{1,0:T(8,128)(2,1)}, bf16[57...) custom-call(bf16[192,512]{1,0:T(8,128)(2,1)} %x_ref.1, ...), custom_call_target="tpu_custom_call" | custom-call | tf_op jit(solution)/shard_map/dispatch/pallas_call | solution.py:590
  62.5 0.1 collective-permute-start
  62.6 1.5 %collective-permute-start.1 = (bf16[576,512]{1,0:T(8,128)(2,1)}, bf16[576,512]{1,0:T(8,128)(2,1)S(1)}, u32[]{:S(2)}, u32[]{:S(2)}) collective-permute-start(bf16[576,512]{1,0:T(8,128)(2,1)} %get-tuple-element.31), channel_id=1, source_target_pairs={{0,3},{1,0},{2,1},{3,2},{4,7},{5,4},{6,5},{7,6},{8,11},{9,8},{10,9... | collective-permute-start | bytes 1769480 | tf_op jit(solution)/shard_map/ppermute | solution.py:1044
  64.0 0.0 copy-done.13
  64.0 0.1 copy.20.routes_ref
  64.1 0.0 copy-start.9
  64.1 1.7 %copy-done.9 = bf16[576,2048]{1,0:T(8,128)(2,1)S(1)} copy-done((bf16[576,2048]{1,0:T(8,128)(2,1)S(1)}, bf16[576,2048]{1,0:T(8,128)(2,1)}, u32[]{:S(2)}) %copy-start.9) | copy-done | bytes 2359320
  65.8 1.2 %copy-done.12 = bf16[576,896]{1,0:T(8,128)(2,1)S(1)} copy-done((bf16[576,896]{1,0:T(8,128)(2,1)S(1)}, bf16[576,896]{1,0:T(8,128)(2,1)}, u32[]{:S(2)}) %copy-start.12) | copy-done | bytes 1032216
  67.0 5.0 %grads_from.1 = bf16[896,2048]{1,0:T(8,128)(2,1)} custom-call(bf16[576,896]{1,0:T(8,128)(2,1)S(1)} %copy-done.12, bf16[576,2048]{1,0:T(8,128)(2,1)S(1)} %copy-done.9), custom_call_target="tpu_custom_call" | custom-call | flops 2113929216 | bytes 7061504 | tf_op jit(solution)/shard_map/grads_from/pallas_call | solution.py:996
  72.1 0.0 copy-done.8
  72.1 0.0 copy-done.10
  72.1 0.0 copy-done.11
  72.1 0.0 copy-start
  72.1 0.0 copy-start.1
  72.1 0.0 copy-start.2
  72.1 0.0 copy-start.3
  72.1 0.0 copy-start.4
  72.1 0.0 copy-start.5
  72.1 0.0 copy-start.6
  72.2 0.0 copy-start.7
  72.2 8.2 %grads_into.1 = (bf16[2048,896]{1,0:T(8,128)(2,1)}, bf16[2048,896]{1,0:T(8,128)(2,1)}) custom-call(bf16[576,2048]{1,0:T(8,128)(2,1)S(1)} %copy-done.8, bf16[576,896]{1,0:T(8,128)(2,1)S(1)} %copy-done.10, bf16[576,896]{1,0:T(8,128)(2,1)S(1)} %copy-done.11), custom_call_target="tpu_custom_call" | custom-call | flops 4227858432 | bytes 11763712 | tf_op jit(solution)/shard_map/grads_into/pallas_call | solution.py:986
  80.4 0.0 collective-permute-done.fwd_ref
  80.4 0.0 collective-permute-done.1.bwd_ref
  80.4 0.0 copy-done
  80.4 0.0 copy-done.1
  80.4 0.0 copy-done.2
  80.4 0.0 copy-done.3
  80.5 37.8 %tail.1 = (f32[64,256]{1,0:T(8,128)S(1)}, f32[192,256]{1,0:T(8,128)S(1)}, f32[192,256]{1,0:T(8,128)S(1)}) custom-call(bf16[576,512]{1,0:T(8,128)(2,1)S(1)} %copy-done.5, bf16[576,512]{1,0:T(8,128)(2,1)S(1)} %collective-permute-done.fwd_ref, bf16[576,512]{1,0:T(8,128)(2,1)S(1)} %collective-permute-done.1.bwd_ref, bf16[192,512]{1,0:T(8,128)(2,1)S(1)} %copy-done.4, ...), custom_call_target="tpu_custom_call" | custom-call | tf_op jit(solution)/shard_map/tail/pallas_call | solution.py:920
  118.3 0.6 copy.24
  118.9 0.7 copy.25
  119.6 0.7 copy.26
  (8 shorter events, 0.0 us)
Async XLA Ops:
  0.6 63.4 %copy-start.13 = (s32[192,2]{0,1:T(2,128)S(1)}, s32[192,2]{0,1:T(2,128)}, u32[]{:S(2)}) copy-start(s32[192,2]{0,1:T(2,128)} %param.16) | copy-start | bytes 4612
  62.5 17.9 %collective-permute-start = (bf16[576,512]{1,0:T(8,128)(2,1)}, bf16[576,512]{1,0:T(8,128)(2,1)S(1)}, u32[]{:S(2)}, u32[]{:S(2)}) collective-permute-start(bf16[576,512]{1,0:T(8,128)(2,1)} %get-tuple-element.30), channel_id=1, source_target_pairs={{0,1},{1,2},{2,3},{3,0},{4,5},{5,6},{6,7},{7,4},{8,9},{9,10},{10,1... | collective-permute-start | bytes 1769480 | tf_op jit(solution)/shard_map/ppermute | solution.py:1043
  62.6 17.8 %collective-permute-start.1 = (bf16[576,512]{1,0:T(8,128)(2,1)}, bf16[576,512]{1,0:T(8,128)(2,1)S(1)}, u32[]{:S(2)}, u32[]{:S(2)}) collective-permute-start(bf16[576,512]{1,0:T(8,128)(2,1)} %get-tuple-element.31), channel_id=1, source_target_pairs={{0,3},{1,0},{2,1},{3,2},{4,7},{5,4},{6,5},{7,6},{8,11},{9,8},{10,9... | collective-permute-start | bytes 1769480 | tf_op jit(solution)/shard_map/ppermute | solution.py:1044
  64.1 1.7 %copy-start.9 = (bf16[576,2048]{1,0:T(8,128)(2,1)S(1)}, bf16[576,2048]{1,0:T(8,128)(2,1)}, u32[]{:S(2)}) copy-start(bf16[576,2048]{1,0:T(8,128)(2,1)} %get-tuple-element.28.c_ref) | copy-start | bytes 7077892
  65.8 1.2 %copy-start.12 = (bf16[576,896]{1,0:T(8,128)(2,1)S(1)}, bf16[576,896]{1,0:T(8,128)(2,1)}, u32[]{:S(2)}) copy-start(bf16[576,896]{1,0:T(8,128)(2,1)} %get-tuple-element.27.h_ref) | copy-start | bytes 3096580
  67.0 5.0 %copy-start.8 = (bf16[576,2048]{1,0:T(8,128)(2,1)S(1)}, bf16[576,2048]{1,0:T(8,128)(2,1)}, u32[]{:S(2)}) copy-start(bf16[576,2048]{1,0:T(8,128)(2,1)} %get-tuple-element.22.x_ref) | copy-start | bytes 7077892
  67.0 5.0 %copy-start.10 = (bf16[576,896]{1,0:T(8,128)(2,1)S(1)}, bf16[576,896]{1,0:T(8,128)(2,1)}, u32[]{:S(2)}) copy-start(bf16[576,896]{1,0:T(8,128)(2,1)} %get-tuple-element.23.dg_ref) | copy-start | bytes 3096580
  67.0 5.0 %copy-start.11 = (bf16[576,896]{1,0:T(8,128)(2,1)S(1)}, bf16[576,896]{1,0:T(8,128)(2,1)}, u32[]{:S(2)}) copy-start(bf16[576,896]{1,0:T(8,128)(2,1)} %get-tuple-element.24.du_ref) | copy-start | bytes 3096580
  72.1 8.3 %copy-start = (f32[6,192,256]{2,1,0:T(8,128)S(1)}, f32[6,192,256]{2,1,0:T(8,128)}, u32[]{:S(2)}) copy-start(f32[6,192,256]{2,1,0:T(8,128)} %get-tuple-element.32.rec_ref) | copy-start | bytes 3538948
  72.1 8.3 %copy-start.1 = (bf16[2048,256]{1,0:T(8,128)(2,1)S(1)}, bf16[2048,256]{1,0:T(8,128)(2,1)}, u32[]{:S(2)}) copy-start(bf16[2048,256]{1,0:T(8,128)(2,1)} %wout_ref.1) | copy-start | bytes 3145732
  72.1 8.3 %copy-start.2 = (bf16[8,128,128]{2,1,0:T(8,128)(2,1)S(1)}, bf16[8,128,128]{2,1,0:T(8,128)(2,1)}, u32[]{:S(2)}) copy-start(bf16[8,128,128]{2,1,0:T(8,128)(2,1)} %wr_ref.3) | copy-start | bytes 786436
  72.1 8.3 %copy-start.3 = (bf16[8,128,128]{2,1,0:T(8,128)(2,1)S(1)}, bf16[8,128,128]{2,1,0:T(8,128)(2,1)}, u32[]{:S(2)}) copy-start(bf16[8,128,128]{2,1,0:T(8,128)(2,1)} %wi_ref.3) | copy-start | bytes 786436
  72.1 8.3 %copy-start.4 = (bf16[192,512]{1,0:T(8,128)(2,1)S(1)}, bf16[192,512]{1,0:T(8,128)(2,1)}, u32[]{:S(2)}) copy-start(bf16[192,512]{1,0:T(8,128)(2,1)} %og_ref.1) | copy-start | bytes 589828
  72.1 8.3 %copy-start.5 = (bf16[576,512]{1,0:T(8,128)(2,1)S(1)}, bf16[576,512]{1,0:T(8,128)(2,1)}, u32[]{:S(2)}) copy-start(bf16[576,512]{1,0:T(8,128)(2,1)} %get-tuple-element.29.own_ref) | copy-start | bytes 1769476
  72.1 8.3 %copy-start.6 = (bf16[192,256]{1,0:T(8,128)(2,1)S(1)}, bf16[192,256]{1,0:T(8,128)(2,1)}, u32[]{:S(2)}) copy-start(bf16[192,256]{1,0:T(8,128)(2,1)} %get-tuple-element.33.lru_ref) | copy-start | bytes 294916
  72.2 8.3 %copy-start.7 = (f32[32,2,256]{2,1,0:T(2,128)S(1)}, f32[32,2,256]{2,1,0:T(2,128)}, u32[]{:S(2)}) copy-start(f32[32,2,256]{2,1,0:T(2,128)} %get-tuple-element.34.gain_ref) | copy-start | bytes 196612

commit v4 on v3

--- a/solution.py
+++ b/solution.py
@@ -543,7 +543,13 @@
         back_to(right, lo, hi, to_right)
         back_to(left, lo, hi, to_left)
 
+    def put_acts(lo, hi):
+        rows = pl.ds(lo, hi - lo)
+        for src, dst in ((hid, hid_out), (dg, dg_out), (du, du_out)):
+            put(src.at[rows], dst.at[rows])
+
     finish_far(0)
+    put_acts(0, wide)
     relay(quad)
     relay(quad + 1)
     finish_near(0)
@@ -556,9 +562,7 @@
     finish_far(1)
     for c in crossing[2:]:
         c[0].start()
-    put(hid, hid_out)
-    put(dg, dg_out)
-    put(du, du_out)
+    put_acts(wide, slots)
     finish_near(1)
     put(own_sum, own_out)
     for c, n, lo, hi in crossing:
@@ -569,8 +573,9 @@
         total[lo:hi, :] = (
             (right_dx if n == 0 else left_dx)[lo:hi, :] + far_in[lo:hi, :].astype(F32)
         ).astype(BF16)
-    put(fwd_sum, fwd_out)
-    put(bwd_sum, bwd_out)
+        rows = pl.ds(lo, hi - lo)
+        put(fwd_sum.at[rows], fwd_out.at[rows])
+        put(bwd_sum.at[rows], bwd_out.at[rows])
     for c in outs:
         c.wait()
     for c in first_hop + next_hop + sends + told + started + [c[0] for c in crossing]:
@@ -640,7 +645,7 @@
             pltpu.VMEM((6, tokens, chans), F32),
             pltpu.VMEM((tokens, chans), BF16),
             dma((3,)),
-            dma((11,)),
+            dma((20,)),
             dma((4,)),
             dma((4,)),
             dma((n_sp,)),

time: 120 us -> 120 us (level)
  no operation moved by 1% of the time
where the time goes in v4:
time: 120 us
  Pallas kernels  113 us (94%)
  local copies, waits for them, and re-layouts  5.04 us (4%)
  starting transfers between devices  1.53 us (1%)
    pallas_call x1, Pallas kernels, dispatch(): pl.pallas_call(functools.partial(dispatch_kernel, n_sp), out_shape=(shape...  61.7 us
    pallas_call x1, Pallas kernels, tail(): pl.pallas_call(functools.partial(tail_kernel, n_sp), out_shape=(jax.Shape...  37.8 us
    pallas_call x1, Pallas kernels, weight_gradients(): pl.pallas_call(into_weights_kernel, grid=(width // block,), out_shape=(ja...  8.23 us
    unnamed x32, local copies, waits for them, and re-layouts  5.04 us
    pallas_call x1, Pallas kernels, weight_gradients(): pl.pallas_call(from_weights_kernel, grid=(width // block,), out_shape=jax...  5.03 us
  transfers between devices with their start and end apart: 2, of which 0 were waited for; matrix products, arithmetic and copies ran while one was open for 0% of the time, Pallas kernels for 11%

profile of v4, /device:TPU:27, one launch (start us, length us, event | category | flops | bytes accessed | tf_op | source)
XLA Modules:
  0.0 120.1 jit_solution(1539336380241997806)
XLA Ops:
  0.6 0.0 copy-start.13
  0.6 61.7 %dispatch.1 = (bf16[576,2048]{1,0:T(8,128)(2,1)}, bf16[576,2048]{1,0:T(8,128)(2,1)}, bf16[576,896]{1,0:T(8,128)(2,1)}, bf16[576,896]{1,0:T(8,128)(2,1)}, bf16[57...) custom-call(bf16[192,512]{1,0:T(8,128)(2,1)} %x_ref.1, ...), custom_call_target="tpu_custom_call" | custom-call | tf_op jit(solution)/shard_map/dispatch/pallas_call | solution.py:595
  62.4 0.1 collective-permute-start
  62.4 1.5 %collective-permute-start.1 = (bf16[576,512]{1,0:T(8,128)(2,1)}, bf16[576,512]{1,0:T(8,128)(2,1)S(1)}, u32[]{:S(2)}, u32[]{:S(2)}) collective-permute-start(bf16[576,512]{1,0:T(8,128)(2,1)} %get-tuple-element.31), channel_id=1, source_target_pairs={{0,3},{1,0},{2,1},{3,2},{4,7},{5,4},{6,5},{7,6},{8,11},{9,8},{10,9... | collective-permute-start | bytes 1769480 | tf_op jit(solution)/shard_map/ppermute | solution.py:1049
  63.9 0.0 copy-done.13
  63.9 0.1 copy.20.routes_ref
  64.0 0.0 copy-start.9
  64.0 1.7 %copy-done.9 = bf16[576,2048]{1,0:T(8,128)(2,1)S(1)} copy-done((bf16[576,2048]{1,0:T(8,128)(2,1)S(1)}, bf16[576,2048]{1,0:T(8,128)(2,1)}, u32[]{:S(2)}) %copy-start.9) | copy-done | bytes 2359320
  65.7 1.2 %copy-done.12 = bf16[576,896]{1,0:T(8,128)(2,1)S(1)} copy-done((bf16[576,896]{1,0:T(8,128)(2,1)S(1)}, bf16[576,896]{1,0:T(8,128)(2,1)}, u32[]{:S(2)}) %copy-start.12) | copy-done | bytes 1032216
  66.9 5.0 %grads_from.1 = bf16[896,2048]{1,0:T(8,128)(2,1)} custom-call(bf16[576,896]{1,0:T(8,128)(2,1)S(1)} %copy-done.12, bf16[576,2048]{1,0:T(8,128)(2,1)S(1)} %copy-done.9), custom_call_target="tpu_custom_call" | custom-call | flops 2113929216 | bytes 7061504 | tf_op jit(solution)/shard_map/grads_from/pallas_call | solution.py:1001
  72.0 0.0 copy-done.8
  72.0 0.0 copy-done.10
  72.0 0.0 copy-done.11
  72.0 0.0 copy-start
  72.0 0.0 copy-start.1
  72.0 0.0 copy-start.2
  72.0 0.0 copy-start.3
  72.0 0.0 copy-start.4
  72.0 0.0 copy-start.5
  72.0 0.0 copy-start.6
  72.0 0.0 copy-start.7
  72.1 8.2 %grads_into.1 = (bf16[2048,896]{1,0:T(8,128)(2,1)}, bf16[2048,896]{1,0:T(8,128)(2,1)}) custom-call(bf16[576,2048]{1,0:T(8,128)(2,1)S(1)} %copy-done.8, bf16[576,896]{1,0:T(8,128)(2,1)S(1)} %copy-done.10, bf16[576,896]{1,0:T(8,128)(2,1)S(1)} %copy-done.11), custom_call_target="tpu_custom_call" | custom-call | flops 4227858432 | bytes 11763712 | tf_op jit(solution)/shard_map/grads_into/pallas_call | solution.py:991
  80.3 0.0 collective-permute-done.fwd_ref
  80.3 0.0 collective-permute-done.1.bwd_ref
  80.3 0.0 copy-done
  80.3 0.0 copy-done.1
  80.3 0.0 copy-done.2
  80.3 0.0 copy-done.3
  80.4 37.8 %tail.1 = (f32[64,256]{1,0:T(8,128)S(1)}, f32[192,256]{1,0:T(8,128)S(1)}, f32[192,256]{1,0:T(8,128)S(1)}) custom-call(bf16[576,512]{1,0:T(8,128)(2,1)S(1)} %copy-done.5, bf16[576,512]{1,0:T(8,128)(2,1)S(1)} %collective-permute-done.fwd_ref, bf16[576,512]{1,0:T(8,128)(2,1)S(1)} %collective-permute-done.1.bwd_ref, bf16[192,512]{1,0:T(8,128)(2,1)S(1)} %copy-done.4, ...), custom_call_target="tpu_custom_call" | custom-call | tf_op jit(solution)/shard_map/tail/pallas_call | solution.py:925
  118.2 0.6 copy.24
  118.8 0.7 copy.25
  119.5 0.7 copy.26
  (8 shorter events, 0.0 us)
Async XLA Ops:
  0.6 63.3 %copy-start.13 = (s32[192,2]{0,1:T(2,128)S(1)}, s32[192,2]{0,1:T(2,128)}, u32[]{:S(2)}) copy-start(s32[192,2]{0,1:T(2,128)} %param.16) | copy-start | bytes 4612
  62.4 17.9 %collective-permute-start = (bf16[576,512]{1,0:T(8,128)(2,1)}, bf16[576,512]{1,0:T(8,128)(2,1)S(1)}, u32[]{:S(2)}, u32[]{:S(2)}) collective-permute-start(bf16[576,512]{1,0:T(8,128)(2,1)} %get-tuple-element.30), channel_id=1, source_target_pairs={{0,1},{1,2},{2,3},{3,0},{4,5},{5,6},{6,7},{7,4},{8,9},{9,10},{10,1... | collective-permute-start | bytes 1769480 | tf_op jit(solution)/shard_map/ppermute | solution.py:1048
  62.4 17.8 %collective-permute-start.1 = (bf16[576,512]{1,0:T(8,128)(2,1)}, bf16[576,512]{1,0:T(8,128)(2,1)S(1)}, u32[]{:S(2)}, u32[]{:S(2)}) collective-permute-start(bf16[576,512]{1,0:T(8,128)(2,1)} %get-tuple-element.31), channel_id=1, source_target_pairs={{0,3},{1,0},{2,1},{3,2},{4,7},{5,4},{6,5},{7,6},{8,11},{9,8},{10,9... | collective-permute-start | bytes 1769480 | tf_op jit(solution)/shard_map/ppermute | solution.py:1049
  64.0 1.7 %copy-start.9 = (bf16[576,2048]{1,0:T(8,128)(2,1)S(1)}, bf16[576,2048]{1,0:T(8,128)(2,1)}, u32[]{:S(2)}) copy-start(bf16[576,2048]{1,0:T(8,128)(2,1)} %get-tuple-element.28.c_ref) | copy-start | bytes 7077892
  65.7 1.2 %copy-start.12 = (bf16[576,896]{1,0:T(8,128)(2,1)S(1)}, bf16[576,896]{1,0:T(8,128)(2,1)}, u32[]{:S(2)}) copy-start(bf16[576,896]{1,0:T(8,128)(2,1)} %get-tuple-element.27.h_ref) | copy-start | bytes 3096580
  66.9 5.0 %copy-start.8 = (bf16[576,2048]{1,0:T(8,128)(2,1)S(1)}, bf16[576,2048]{1,0:T(8,128)(2,1)}, u32[]{:S(2)}) copy-start(bf16[576,2048]{1,0:T(8,128)(2,1)} %get-tuple-element.22.x_ref) | copy-start | bytes 7077892
  66.9 5.0 %copy-start.10 = (bf16[576,896]{1,0:T(8,128)(2,1)S(1)}, bf16[576,896]{1,0:T(8,128)(2,1)}, u32[]{:S(2)}) copy-start(bf16[576,896]{1,0:T(8,128)(2,1)} %get-tuple-element.23.dg_ref) | copy-start | bytes 3096580
  66.9 5.0 %copy-start.11 = (bf16[576,896]{1,0:T(8,128)(2,1)S(1)}, bf16[576,896]{1,0:T(8,128)(2,1)}, u32[]{:S(2)}) copy-start(bf16[576,896]{1,0:T(8,128)(2,1)} %get-tuple-element.24.du_ref) | copy-start | bytes 3096580
  72.0 8.3 %copy-start = (f32[6,192,256]{2,1,0:T(8,128)S(1)}, f32[6,192,256]{2,1,0:T(8,128)}, u32[]{:S(2)}) copy-start(f32[6,192,256]{2,1,0:T(8,128)} %get-tuple-element.32.rec_ref) | copy-start | bytes 3538948
  72.0 8.3 %copy-start.1 = (bf16[2048,256]{1,0:T(8,128)(2,1)S(1)}, bf16[2048,256]{1,0:T(8,128)(2,1)}, u32[]{:S(2)}) copy-start(bf16[2048,256]{1,0:T(8,128)(2,1)} %wout_ref.1) | copy-start | bytes 3145732
  72.0 8.3 %copy-start.2 = (bf16[8,128,128]{2,1,0:T(8,128)(2,1)S(1)}, bf16[8,128,128]{2,1,0:T(8,128)(2,1)}, u32[]{:S(2)}) copy-start(bf16[8,128,128]{2,1,0:T(8,128)(2,1)} %wr_ref.3) | copy-start | bytes 786436
  72.0 8.3 %copy-start.3 = (bf16[8,128,128]{2,1,0:T(8,128)(2,1)S(1)}, bf16[8,128,128]{2,1,0:T(8,128)(2,1)}, u32[]{:S(2)}) copy-start(bf16[8,128,128]{2,1,0:T(8,128)(2,1)} %wi_ref.3) | copy-start | bytes 786436
  72.0 8.3 %copy-start.4 = (bf16[192,512]{1,0:T(8,128)(2,1)S(1)}, bf16[192,512]{1,0:T(8,128)(2,1)}, u32[]{:S(2)}) copy-start(bf16[192,512]{1,0:T(8,128)(2,1)} %og_ref.1) | copy-start | bytes 589828
  72.0 8.3 %copy-start.5 = (bf16[576,512]{1,0:T(8,128)(2,1)S(1)}, bf16[576,512]{1,0:T(8,128)(2,1)}, u32[]{:S(2)}) copy-start(bf16[576,512]{1,0:T(8,128)(2,1)} %get-tuple-element.29.own_ref) | copy-start | bytes 1769476
  72.0 8.3 %copy-start.6 = (bf16[192,256]{1,0:T(8,128)(2,1)S(1)}, bf16[192,256]{1,0:T(8,128)(2,1)}, u32[]{:S(2)}) copy-start(bf16[192,256]{1,0:T(8,128)(2,1)} %get-tuple-element.33.lru_ref) | copy-start | bytes 294916
  72.0 8.3 %copy-start.7 = (f32[32,2,256]{2,1,0:T(2,128)S(1)}, f32[32,2,256]{2,1,0:T(2,128)}, u32[]{:S(2)}) copy-start(f32[32,2,256]{2,1,0:T(2,128)} %get-tuple-element.34.gain_ref) | copy-start | bytes 196612
